TPU v7x, 256 devices: a whole 4x4x8 slice. The times are simulated.
256 devices in a mesh: ep: 64 (over z, x, core), tp: 4 (over y).
Axes of the slice: x: 4, y: 4, z: 8, core: 2. Of those that a mesh axis runs over, the one named last changes fastest.
Arguments:
- tokens: bfloat16 [32768, 4096], P('ep', 'tp'), may hold values from -100 to 100, as said below
- routes: int32 [32768, 2], P('ep'), may hold values from 0 to 127, all different within a row; in each aligned block of 512 rows (0 to 511, 512 to 1023, ...) at most 16 rows name the same one
- route_weights: float32 [32768, 2], P('ep'), may hold values from 0.1 to 1
- norm_gain: float32 [4096], P('tp'), may hold values from 0.1 to 1.9
- gate_weight: bfloat16 [128, 4096, 512], P('ep', 'tp'), may hold values from -0.09375 to 0.09375
- up_weight: bfloat16 [128, 4096, 512], P('ep', 'tp'), may hold values from -0.09375 to 0.09375
- down_weight: bfloat16 [128, 512, 4096], P('ep', None, 'tp'), may hold values from -0.25 to 0.25
- final_gain: float32 [4096], P('tp'), may hold values from 0.1 to 1.9
Outputs:
- mixed: bfloat16 [32768, 4096], P('ep', 'tp')
Inputs may be any that keep to these rules, and one draw needn't show every extreme that they name: `tokens`: real-valued activations whose features differ in scale. `routes`: each row names 2 different experts; among the 512 rows of one aligned block no expert is named more than 16 times, a bound that some block reaches.
All inputs are finite; a program needn't handle non-finite values.
Results may differ from a plain program's by a relative error of at most 0.018.
Values may be sent and summed in bfloat16 or wider, within the bound.
A program may use at most 64 MiB of HBM per device.

v0:
```python
import jax
import jax.numpy as jnp
from jax import lax
from jax.sharding import PartitionSpec as P

D = 4096


EPSILON = 1e-06


def in_blocks(x, dim, peers):
    before, after = (x.shape[:dim], x.shape[dim + 1 :])
    return jnp.moveaxis(x.reshape(*before, peers, -1, *after), dim, 0)


def sent_and_summed(x, axis, dim):
    peers = lax.axis_size(axis)
    tiles = lax.all_to_all(in_blocks(x, dim, peers), axis, 0, 0, tiled=True)
    return jnp.sum(tiles.astype(jnp.float32), axis=0)


def side_by_side(arrays, axis, dim, along):
    ends, at = ([], 0)
    for a in arrays[:-1]:
        at += a.shape[along]
        ends.append(at)
    both = jnp.concatenate(arrays, axis=along)
    return tuple(jnp.split(sent_and_summed(both, axis, dim), ends, axis=along))


def from_everyone(x, axis):
    copies = jnp.broadcast_to(x, (lax.axis_size(axis), *x.shape))
    return lax.all_to_all(copies, axis, split_axis=0, concat_axis=0, tiled=True)


def joined_along(tiles, dim):
    dims = list(tiles.shape[1:])
    dims[dim] *= tiles.shape[0]
    return jnp.moveaxis(tiles, 0, dim).reshape(dims)


def collect(x, axis, dim):
    tiles = from_everyone(x, axis)
    return joined_along(tiles, dim)


def taken_together(x, axis):
    everything = from_everyone(x, axis)
    return jnp.sum(everything, axis=0)


def expert_rows(weights, block):
    w_gate, w_up, w_down = weights
    gate = jnp.einsum("scd,df->scf", block, w_gate, preferred_element_type=jnp.float32)
    upper = jnp.einsum("scd,df->scf", block, w_up, preferred_element_type=jnp.float32)
    gate_sum, upper_sum = side_by_side(
        (gate.astype(jnp.bfloat16), upper.astype(jnp.bfloat16)), "tp", 2, 0
    )
    share = (jax.nn.silu(gate_sum) * upper_sum).astype(jnp.bfloat16)
    hidden = collect(share, "tp", 2)
    return jnp.einsum("scf,fd->scd", hidden, w_down, preferred_element_type=jnp.float32).astype(
        jnp.bfloat16
    )


def serve_all(weight_list, block):
    results = [
        expert_rows(weight_list[member], block[:, member]) for member in range(len(weight_list))
    ]
    return lax.all_to_all(jnp.stack(results, axis=1), "ep", split_axis=0, concat_axis=0, tiled=True)


def body(tokens, routes, route_weights, norm_gain, gate_weight, up_weight, down_weight, final_gain):
    ep_count = lax.axis_size("ep")
    local_count = gate_weight.shape[0]
    experts = ep_count * local_count
    tok_rows = tokens.shape[0]
    top_count = routes.shape[1]
    capacity = 4 * tok_rows // experts
    values = tokens.astype(jnp.float32)
    squares = taken_together(jnp.sum(values * values, axis=-1), "tp")
    normed = (values * lax.rsqrt(squares / D + EPSILON)[:, None] * norm_gain).astype(jnp.bfloat16)
    chosen = routes.reshape(-1)
    onehot = (chosen[:, None] == jnp.arange(experts, dtype=jnp.int32)[None, :]).astype(jnp.int32)
    slots = jnp.sum((jnp.cumsum(onehot, axis=0) - onehot) * onehot, axis=1)
    target = chosen * capacity + slots
    owners = jnp.arange(tok_rows * top_count, dtype=jnp.int32) // top_count
    table = jnp.full((experts * capacity,), tok_rows, jnp.int32).at[target].set(owners)
    padded = jnp.concatenate([normed, jnp.zeros((1, normed.shape[1]), jnp.bfloat16)], axis=0)
    outgoing = padded[table].reshape(ep_count, local_count, capacity, normed.shape[1])
    weight_list = [
        (gate_weight[member], up_weight[member], down_weight[member])
        for member in range(local_count)
    ]
    arrived = serve_all(
        weight_list, lax.all_to_all(outgoing, "ep", split_axis=0, concat_axis=0, tiled=True)
    )
    returned = arrived.reshape(experts * capacity, normed.shape[1])
    position = target.reshape(tok_rows, top_count)
    combined = jnp.zeros((tok_rows, normed.shape[1]), jnp.float32)
    for which in range(top_count):
        combined = combined + route_weights[:, which : which + 1] * returned[
            position[:, which]
        ].astype(jnp.float32)
    closing = taken_together(jnp.sum(combined * combined, axis=-1), "tp")
    return (combined * lax.rsqrt(closing / D + EPSILON)[:, None] * final_gain).astype(jnp.bfloat16)


def solution(mesh):
    in_specs = (
        P("ep", "tp"),
        P("ep", None),
        P("ep", None),
        P("tp"),
        P("ep", "tp", None),
        P("ep", "tp", None),
        P("ep", None, "tp"),
        P("tp"),
    )
    out_specs = P("ep", "tp")
    return jax.shard_map(body, mesh=mesh, in_specs=in_specs, out_specs=out_specs, check_vma=False)
```

profile of v0, /device:TPU:36, one launch (start us, length us, event | category | flops | bytes accessed | tf_op | source)
XLA Modules:
  0.0 365.5 jit_solution(13011418187434321295)
XLA Ops:
  2.1 4.5 %all-to-all-start = ((f32[4,1,512]{2,1,0:T(1,128)}), f32[4,1,512]{2,1,0:T(1,128)S(1)}, u32[]{:S(2)}, u32[]{:S(2)}) async-start(f32[4,1,512]{2,1,0:T(1,128)} %broadcast_in_dim.12), calls=%async_computation | async-start | bytes 16384 | tf_op jit(solution)/shard_map/all_to_all | solution.py:34
  9.1 4.3 %scatter_custom_fusion = s32[2048]{0:T(1024)S(1)} fusion(s32[1024]{0:T(1024)S(1)} %bitcast.101, s32[1024]{0:T(1024)S(1)} %add_select_fusion, s32[]{:T(128)} %constant.39.clone.1), kind=kCustom, calls=%fused_computation.77 | custom fusion | bytes 8196 | tf_op jit(solution)/shard_map/scatter | solution.py:89
  13.9 9.7 %gather_fusion = bf16[2048,1024]{1,0:T(8,128)(2,1)} fusion(bf16[513,1024]{1,0:T(8,128)(2,1)S(1)} %concatenate.9, s32[2048]{0:T(1024)S(1)} %fusion.36), kind=kCustom, calls=%fused_computation | custom fusion | bytes 8396800 | tf_op jit(solution)/shard_map/gather | solution.py:91
  23.6 107.0 %all_to_all.42 = bf16[64,2,16,1024]{3,2,1,0:T(8,128)(2,1)S(1)} all-to-all(bf16[64,2,16,1024]{3,2,1,0:T(8,128)(2,1)} %bitcast.95), channel_id=1, replica_groups=mesh['ep'=64,'tp'=4] {'ep'}, dimensions={0} | all-to-all | bytes 8388608 | tf_op jit(solution)/shard_map/all_to_all | solution.py:97
  134.9 1.7 bitcast_bitcast_fusion.1
  136.6 4.8 %all-to-all-start.2 = ((bf16[4,128,16,128]{3,2,1,0:T(8,128)(2,1)}), bf16[4,128,16,128]{3,2,1,0:T(8,128)(2,1)S(1)}, u32[]{:S(2)}, u32[]{:S(2)}) async-start(bf16[4,128,16,128]{3,2,1,0:T(8,128)(2,1)} %bitcast_bitcast_fusion.1), calls=%async_computation.2 | async-start | bytes 4194304 | tf_op jit(solution)/shard_map/all_to_all | solution.py:19
  141.4 3.2 fusion.8
  146.5 1.7 bitcast_bitcast_fusion
  148.2 19.2 %all-to-all-done.2 = bf16[4,128,16,128]{3,2,1,0:T(8,128)(2,1)S(1)} async-done(((bf16[4,128,16,128]{3,2,1,0:T(8,128)(2,1)}), bf16[4,128,16,128]{3,2,1,0:T(8,128)(2,1)S(1)}, u32[]{:S(2)}, u32[]{:S(2)}) %all-to-all-start.2) | async-done | bytes 2097184 | tf_op jit(solution)/shard_map/all_to_all | solution.py:19
  167.4 4.4 %all-to-all-start.4 = ((bf16[4,128,16,128]{3,2,1,0:T(8,128)(2,1)}), bf16[4,128,16,128]{3,2,1,0:T(8,128)(2,1)}, u32[]{:S(2)}, u32[]{:S(2)}) async-start(bf16[4,128,16,128]{3,2,1,0:T(8,128)(2,1)} %bitcast_bitcast_fusion), calls=%async_computation.4 | async-start | bytes 4194304 | tf_op jit(solution)/shard_map/all_to_all | solution.py:19
  172.3 24.7 %all-to-all-done.4 = bf16[4,128,16,128]{3,2,1,0:T(8,128)(2,1)} async-done(((bf16[4,128,16,128]{3,2,1,0:T(8,128)(2,1)}), bf16[4,128,16,128]{3,2,1,0:T(8,128)(2,1)}, u32[]{:S(2)}, u32[]{:S(2)}) %all-to-all-start.4) | async-done | bytes 2097184 | tf_op jit(solution)/shard_map/all_to_all | solution.py:19
  198.1 3.5 all-to-all-start.3
  201.6 2.0 convert_reduce_fusion
  203.8 10.8 %all-to-all-done.3 = bf16[4,64,16,128]{3,2,1,0:T(8,128)(2,1)S(1)} async-done(((bf16[4,64,16,128]{3,2,1,0:T(8,128)(2,1)}), bf16[4,64,16,128]{3,2,1,0:T(8,128)(2,1)S(1)}, u32[]{:S(2)}, u32[]{:S(2)}) %all-to-all-start.3) | async-done | bytes 1048608 | tf_op jit(solution)/shard_map/all_to_all | solution.py:34
  215.7 4.4 %all-to-all-start.5 = ((bf16[4,64,16,128]{3,2,1,0:T(8,128)(2,1)}), bf16[4,64,16,128]{3,2,1,0:T(8,128)(2,1)}, u32[]{:S(2)}, u32[]{:S(2)}) async-start(bf16[4,64,16,128]{3,2,1,0:T(8,128)(2,1)} %broadcast_in_dim.31), calls=%async_computation.5 | async-start | bytes 2097152 | tf_op jit(solution)/shard_map/all_to_all | solution.py:34
  220.1 2.5 convert_bitcast_fusion.1
  222.6 9.2 %all-to-all-done.5 = bf16[4,64,16,128]{3,2,1,0:T(8,128)(2,1)} async-done(((bf16[4,64,16,128]{3,2,1,0:T(8,128)(2,1)}), bf16[4,64,16,128]{3,2,1,0:T(8,128)(2,1)}, u32[]{:S(2)}, u32[]{:S(2)}) %all-to-all-start.5) | async-done | bytes 1048608 | tf_op jit(solution)/shard_map/all_to_all | solution.py:34
  231.9 2.8 convert_bitcast_fusion
  235.0 2.4 copy.59
  237.5 11.9 %all-to-all-start.6 = ((bf16[64,2,16,1024]{3,2,1,0:T(8,128)(2,1)}), bf16[64,2,16,1024]{3,2,1,0:T(8,128)(2,1)}, u32[]{:S(2)}, u32[]{:S(2)}) async-start(bf16[64,2,16,1024]{3,2,1,0:T(8,128)(2,1)} %copy.59), calls=%async_computation.6 | async-start | bytes 8388608 | tf_op jit(solution)/shard_map/all_to_all | solution.py:71
  249.7 94.9 %all-to-all-done.6 = bf16[64,2,16,1024]{3,2,1,0:T(8,128)(2,1)} async-done(((bf16[64,2,16,1024]{3,2,1,0:T(8,128)(2,1)}), bf16[64,2,16,1024]{3,2,1,0:T(8,128)(2,1)}, u32[]{:S(2)}, u32[]{:S(2)}) %all-to-all-start.6) | async-done | bytes 4194336 | tf_op jit(solution)/shard_map/all_to_all | solution.py:71
  344.6 5.5 %gather_fusion.2 = bf16[512,1024]{1,0:T(8,128)(2,1)S(1)} fusion(bf16[2048,1024]{1,0:T(8,128)(2,1)} %bitcast.27, s32[1024]{0:T(1024)S(1)} %get-tuple-element.11), kind=kCustom, calls=%fused_computation.2 | custom fusion | bytes 2099200 | tf_op jit(solution)/shard_map/gather | solution.py:103
  350.1 5.5 %gather_fusion.1 = bf16[512,1024]{1,0:T(8,128)(2,1)S(1)} fusion(bf16[2048,1024]{1,0:T(8,128)(2,1)} %bitcast.27, s32[1024]{0:T(1024)S(1)} %get-tuple-element.12), kind=kCustom, calls=%fused_computation.1 | custom fusion | bytes 2099200 | tf_op jit(solution)/shard_map/gather | solution.py:103
  356.2 7.7 %all_to_all.43 = f32[4,1,512]{2,1,0:T(1,128)S(1)} all-to-all(f32[4,1,512]{2,1,0:T(1,128)S(1)} %broadcast_in_dim.32), channel_id=1, replica_groups=mesh['ep'=64,'tp'=4] {'tp'}, dimensions={0} | all-to-all | bytes 16384 | tf_op jit(solution)/shard_map/all_to_all | solution.py:34
  (59 shorter events, 16.9 us)
Async XLA Ops:
  2.1 11.3 %all-to-all-start = ((f32[4,1,512]{2,1,0:T(1,128)}), f32[4,1,512]{2,1,0:T(1,128)S(1)}, u32[]{:S(2)}, u32[]{:S(2)}) async-start(f32[4,1,512]{2,1,0:T(1,128)} %broadcast_in_dim.12), calls=%async_computation | async-start | bytes 16384 | tf_op jit(solution)/shard_map/all_to_all | solution.py:34
  8.1 5.4 %copy-start = (bf16[512,1024]{1,0:T(8,128)(2,1)S(1)}, bf16[512,1024]{1,0:T(8,128)(2,1)}, u32[]{:S(2)}) copy-start(bf16[512,1024]{1,0:T(8,128)(2,1)} %param.8) | copy-start | bytes 3145732
  8.1 5.4 %copy-start.3 = (f32[1024]{0:T(1024)S(1)}, f32[1024]{0:T(1024)}, u32[]{:S(2)}) copy-start(f32[1024]{0:T(1024)} %param.11) | copy-start | bytes 12292
  23.6 107.0 %copy-start.6 = (bf16[2,1024,512]{2,1,0:T(8,128)(2,1)S(1)}, bf16[2,1024,512]{2,1,0:T(8,128)(2,1)}, u32[]{:S(2)}) copy-start(bf16[2,1024,512]{2,1,0:T(8,128)(2,1)} %param.13) | copy-start | bytes 6291460
  130.6 2.1 copy-start.1
  130.6 3.1 copy-start.7
  136.6 30.7 %all-to-all-start.2 = ((bf16[4,128,16,128]{3,2,1,0:T(8,128)(2,1)}), bf16[4,128,16,128]{3,2,1,0:T(8,128)(2,1)S(1)}, u32[]{:S(2)}, u32[]{:S(2)}) async-start(bf16[4,128,16,128]{3,2,1,0:T(8,128)(2,1)} %bitcast_bitcast_fusion.1), calls=%async_computation.2 | async-start | bytes 4194304 | tf_op jit(solution)/shard_map/all_to_all | solution.py:19
  141.4 3.3 copy-start.2
  141.4 3.8 %copy-start.8 = (bf16[2,1024,512]{2,1,0:T(8,128)(2,1)S(1)}, bf16[2,1024,512]{2,1,0:T(8,128)(2,1)}, u32[]{:S(2)}) copy-start(bf16[2,1024,512]{2,1,0:T(8,128)(2,1)} %param.12) | copy-start | bytes 6291460
  167.4 29.6 %all-to-all-start.4 = ((bf16[4,128,16,128]{3,2,1,0:T(8,128)(2,1)}), bf16[4,128,16,128]{3,2,1,0:T(8,128)(2,1)}, u32[]{:S(2)}, u32[]{:S(2)}) async-start(bf16[4,128,16,128]{3,2,1,0:T(8,128)(2,1)} %bitcast_bitcast_fusion), calls=%async_computation.4 | async-start | bytes 4194304 | tf_op jit(solution)/shard_map/all_to_all | solution.py:19
  198.1 16.5 %all-to-all-start.3 = ((bf16[4,64,16,128]{3,2,1,0:T(8,128)(2,1)}), bf16[4,64,16,128]{3,2,1,0:T(8,128)(2,1)S(1)}, u32[]{:S(2)}, u32[]{:S(2)}) async-start(bf16[4,64,16,128]{3,2,1,0:T(8,128)(2,1)} %broadcast_in_dim.30), calls=%async_computation.3 | async-start | bytes 2097152 | tf_op jit(solution)/shard_map/all_to_all | solution.py:34
  215.7 16.2 %all-to-all-start.5 = ((bf16[4,64,16,128]{3,2,1,0:T(8,128)(2,1)}), bf16[4,64,16,128]{3,2,1,0:T(8,128)(2,1)}, u32[]{:S(2)}, u32[]{:S(2)}) async-start(bf16[4,64,16,128]{3,2,1,0:T(8,128)(2,1)} %broadcast_in_dim.31), calls=%async_computation.5 | async-start | bytes 2097152 | tf_op jit(solution)/shard_map/all_to_all | solution.py:34
  237.5 12.2 %copy-start.5 = (f32[512,2]{0,1:T(2,128)S(1)}, f32[512,2]{0,1:T(2,128)}, u32[]{:S(2)}) copy-start(f32[512,2]{0,1:T(2,128)} %param.10) | copy-start | bytes 12292
  237.5 107.1 %all-to-all-start.6 = ((bf16[64,2,16,1024]{3,2,1,0:T(8,128)(2,1)}), bf16[64,2,16,1024]{3,2,1,0:T(8,128)(2,1)}, u32[]{:S(2)}, u32[]{:S(2)}) async-start(bf16[64,2,16,1024]{3,2,1,0:T(8,128)(2,1)} %copy.59), calls=%async_computation.6 | async-start | bytes 8388608 | tf_op jit(solution)/shard_map/all_to_all | solution.py:71
  355.5 8.4 %copy-start.4 = (f32[1024]{0:T(1024)S(1)}, f32[1024]{0:T(1024)}, u32[]{:S(2)}) copy-start(f32[1024]{0:T(1024)} %param.15) | copy-start | bytes 12292
where the time goes:
time: 368 us; the launch traced here: 365 us
  waiting for transfers between devices  159 us (43%)
  blocking collectives  115 us (31%)
  local copies, waits for them, and re-layouts  34.4 us (9%)
  starting transfers between devices  33.5 us (9%)
  matrix products  12.2 us (3%)
  other arithmetic  11.5 us (3%)
    all_to_all x1, blocking collectives, body(): lax.all_to_all(outgoing, 'ep', split_axis=0, concat_axis=0, tiled=True)  107 us
    all_to_all x1, waiting for transfers between devices, serve_all(): lax.all_to_all(jnp.stack(results, axis=1), 'ep', split_axis=0, concat_axi...  94.9 us
    all_to_all x2, waiting for transfers between devices, sent_and_summed(): tiles = lax.all_to_all(in_blocks(x, dim, peers), axis, 0, 0, tiled=True)  43.9 us
    all_to_all x3, waiting for transfers between devices, from_everyone(): return lax.all_to_all(copies, axis, split_axis=0, concat_axis=0, tiled=True)  20 us
    all_to_all x3, starting transfers between devices, from_everyone(): return lax.all_to_all(copies, axis, split_axis=0, concat_axis=0, tiled=True)  12.4 us
    all_to_all x1, starting transfers between devices, serve_all(): lax.all_to_all(jnp.stack(results, axis=1), 'ep', split_axis=0, concat_axi...  11.9 us
    gather x2, local copies, waits for them, and re-layouts, body(): returned[position[:, which]].astype(jnp.float32)  10.9 us
    gather x1, local copies, waits for them, and re-layouts, body(): padded[table].reshape(ep_count, local_count, capacity, normed.shape[1])  9.67 us
  transfers between devices with their start and end apart: 6, of which 5 were waited for; matrix products, arithmetic and copies ran while one was open for 5% of the time, Pallas kernels for 0%

commit v1 on v0

v1 whole, which is shorter than its diff:
```python
import functools

import jax
import jax.numpy as jnp
from jax import lax
from jax.experimental import pallas as pl
from jax.experimental.pallas import tpu as pltpu
from jax.sharding import PartitionSpec as P

EPSILON = 1e-06
NZ = 8
F32 = jnp.float32
BF16 = jnp.bfloat16
I32 = jnp.int32


def layer_kernel(
    NP, NT, tok, rts, rws, ngain, fgain, gw, uw, dw, out,
    X0, DB, TG, TR, XS, XR, PS, PR, GS, GR, HB, OS, OR, FN, RL, ACC, WGU, WD, SQ, SQ2,
    w_sem, sq_s, sq_r, tg_s, tg_r, db_s, db_r, ps_s, ps_r, x_s, x_r, g_s, g_r, h_s, h_r,
    o_s, o_r, f_s, f_r, rl_s, rl_r,
):
    T, W = tok.shape
    HALF = T // 2
    CAP = TR_CAP(T, NP)
    G2 = 2 * CAP
    RP = NP * G2
    M = NP * CAP
    FQ = WGU.shape[3] // 2
    CB = 256 if W % 256 == 0 else 128
    NB = W // CB
    D = W * NT
    ep = lax.axis_index("ep")
    y = lax.axis_index("tp")
    z = ep // NP
    p = ep % NP

    def zz(o):
        return (z + (o + NZ)) % NZ

    def zdev(o):
        return {"ep": zz(o) * NP + p}

    def pdev(j):
        return {"ep": z * NP + (p + j) % NP}

    def tdev(j):
        return {"tp": (y + j) % NT}

    def send(src, dst, ss, rs, dev):
        pltpu.make_async_remote_copy(
            src_ref=src, dst_ref=dst, send_sem=ss, recv_sem=rs,
            device_id=dev, device_id_type=pl.DeviceIdType.MESH,
        ).start()

    def wait(ref, sem):
        pltpu.make_async_copy(ref, ref, sem).wait()

    barrier = pltpu.get_barrier_semaphore()
    partners = [zdev(o) for o in range(1, NZ)] + [pdev(j) for j in range(1, NP)]
    partners += [tdev(j) for j in range(1, NT)]
    for dev in partners:
        pl.semaphore_signal(barrier, inc=1, device_id=dev, device_id_type=pl.DeviceIdType.MESH)

    for m in range(2):
        for q in range(NT):
            cols = pl.ds(q * FQ, FQ)
            pltpu.make_async_copy(gw.at[m, :, cols], WGU.at[m, q, :, pl.ds(0, FQ)], w_sem.at[0]).start()
            pltpu.make_async_copy(uw.at[m, :, cols], WGU.at[m, q, :, pl.ds(FQ, FQ)], w_sem.at[0]).start()
    pltpu.make_async_copy(dw, WD, w_sem.at[1]).start()

    TB = min(128, T)

    def squares(load, buf):
        for b in range(T // TB):
            v = load(b)
            s = jnp.sum(v * v, axis=1, keepdims=True)
            row = jnp.transpose(jnp.broadcast_to(s, (TB, 128)))
            buf[y, :, b * TB:(b + 1) * TB] = row[0:8, :]

    def share(buf, k):
        for j in range(1, NT):
            send(buf.at[y], buf.at[y], sq_s.at[k], sq_r.at[k], tdev(j))

    def scales(buf, b):
        total = buf[0, :, b * TB:(b + 1) * TB]
        for q in range(1, NT):
            total = total + buf[q, :, b * TB:(b + 1) * TB]
        s = lax.rsqrt(total / D + EPSILON)
        return jnp.transpose(jnp.broadcast_to(s[0:1, :], (128, TB)))

    squares(lambda b: tok[b * TB:(b + 1) * TB, :].astype(F32), SQ)
    pl.semaphore_wait(barrier, len(partners))
    share(SQ, 0)

    r0 = rts[0:1, :]
    r1 = rts[1:2, :]
    NE = NZ * NP * 2
    eio = lax.broadcasted_iota(I32, (NE, T), 0)
    oh0 = jnp.where(eio == r0, 1.0, 0.0)
    oh1 = jnp.where(eio == r1, 1.0, 0.0)
    up = jnp.where(
        lax.broadcasted_iota(I32, (T, T), 0) < lax.broadcasted_iota(I32, (T, T), 1), 1.0, 0.0
    ).astype(BF16)
    before = jnp.dot((oh0 + oh1).astype(BF16), up, preferred_element_type=F32)
    t0 = r0 * CAP + jnp.sum(oh0 * before, axis=0, keepdims=True).astype(I32)
    t1 = r1 * CAP + jnp.sum(oh1 * before, axis=0, keepdims=True).astype(I32)
    TG[...] = jnp.where(lax.broadcasted_iota(I32, (8, T), 0) == 0, t0, t1)
    for slot, o in enumerate((1, -1, 2, -2)):
        send(TG, TR.at[slot], tg_s, tg_r.at[slot], zdev(o))

    wait(SQ.at[pl.ds(0, NT - 1)], sq_r.at[0])
    for h in range(2):
        for b in range(h * HALF // TB, (h + 1) * HALF // TB):
            sc = scales(SQ, b)
            for c in range(W // 128):
                cc = slice(c * 128, (c + 1) * 128)
                v = tok[b * TB:(b + 1) * TB, cc].astype(F32) * sc * ngain[0:1, cc]
                X0[h, b * TB - h * HALF:(b + 1) * TB - h * HALF, cc] = v.astype(BF16)
        send(X0.at[h], DB.at[0, h], db_s.at[0, h], db_r.at[0, h], zdev(1))
        send(X0.at[h], DB.at[1, h], db_s.at[1, h], db_r.at[1, h], zdev(-1))

    def pick(targets, rows, base, xref, dst):
        a = targets[0:1, :]
        b = targets[1:2, :]
        at = lax.broadcasted_iota(I32, (rows, T), 0) + base
        sel = jnp.where((at == a) | (at == b), 1.0, 0.0).astype(BF16)

        def cols(n, carry):
            cc = pl.ds(pl.multiple_of(n * CB, CB), CB)
            got = jnp.dot(sel[:, :HALF], xref[0, :, cc], preferred_element_type=F32)
            got = got + jnp.dot(sel[:, HALF:], xref[1, :, cc], preferred_element_type=F32)
            dst[:, :, cc] = got.astype(BF16).reshape(rows // G2, G2, CB)
            return carry

        lax.fori_loop(0, NB, cols, 0)

    def to_plane(i, src):
        for j in range(1, NP):
            send(src.at[(p + j) % NP], XR.at[i, p], x_s.at[i], x_r.at[i], pdev(j))
        XR[i, p] = src[p]

    def stage_a(i):
        if i == 0:
            pick(TG[...], RP, z * RP, X0, XS.at[0])
        elif i <= 4:
            pick(TR[i - 1], RP, z * RP, DB.at[i - 1], XS.at[i])
        else:
            if i < 7:
                wait(PR.at[i - 5], ps_r.at[i - 5])
            else:
                wait(PR.at[2, pl.ds(0, NP // 2)], ps_r.at[2])
                wait(PR.at[2, pl.ds(NP // 2, NP // 2)], ps_r.at[3])
        to_plane(i, XS.at[i] if i <= 4 else PR.at[i - 5])

    def forward(h):
        wait(DB.at[0, h], db_r.at[0, h])
        send(DB.at[0, h], DB.at[2, h], db_s.at[2, h], db_r.at[2, h], zdev(1))
        wait(DB.at[1, h], db_r.at[1, h])
        send(DB.at[1, h], DB.at[3, h], db_s.at[3, h], db_r.at[3, h], zdev(-1))

    def far(k):
        step = 1 - 2 * k
        for h in range(2):
            wait(DB.at[2 + k, h], db_r.at[2 + k, h])
        wait(TR.at[2 + k], tg_r.at[2 + k])
        pick(TR[2 + k], RP, zz(step) * RP, DB.at[2 + k], PS.at[k, pl.ds(0, NP)])
        send(PS.at[k, pl.ds(0, NP)], PR.at[k], ps_s.at[k, 0], ps_r.at[k], zdev(step))
        H = NP // 2
        pick(TR[2 + k], RP // 2, zz(2 * step) * RP + k * (RP // 2), DB.at[2 + k], PS.at[k, pl.ds(NP, H)])
        send(PS.at[k, pl.ds(NP, H)], PR.at[2, pl.ds(k * H, H)], ps_s.at[k, 1], ps_r.at[2 + k], zdev(2 * step))

    def stage_b(i):
        wait(XR.at[i, pl.ds(0, NP - 1)], x_r.at[i])

        def one(j, carry):
            q = (y + 1 + j) % NT
            for m in range(2):
                rows = XR[i, :, m * CAP:(m + 1) * CAP, :].reshape(M, W)
                got = jnp.dot(rows, WGU[m, q], preferred_element_type=F32)
                GS[i, q, m] = got.astype(BF16)

            @pl.when(j < NT - 1)
            def _():
                send(GS.at[i, q], GR.at[i, y], g_s.at[i], g_r.at[i], {"tp": q})

            return carry

        lax.fori_loop(0, NT, one, 0)

    def stage_c(i):
        wait(GR.at[i, pl.ds(0, NT - 1)], g_r.at[i])
        for m in range(2):
            total = GS[i, y, m].astype(F32)
            for j in range(1, NT):
                total = total + GR[i, (y + j) % NT, m].astype(F32)
            gate = total[:, :FQ]
            HB[i, y, m] = (gate / (1.0 + jnp.exp(-gate)) * total[:, FQ:]).astype(BF16)
        for j in range(1, NT):
            send(HB.at[i, y], HB.at[i, y], h_s.at[i], h_r.at[i], tdev(j))

    def stage_d(i):
        wait(HB.at[i, pl.ds(0, NT - 1)], h_r.at[i])
        for m in range(2):
            hid = jnp.concatenate([HB[i, q, m] for q in range(NT)], axis=1)

            def cols(n, carry):
                cc = pl.ds(pl.multiple_of(n * CB, CB), CB)
                got = jnp.dot(hid, WD[m, :, cc], preferred_element_type=F32)
                OS[i, :, m * CAP:(m + 1) * CAP, cc] = got.astype(BF16).reshape(NP, CAP, CB)
                return carry

            lax.fori_loop(0, NB, cols, 0)
        for j in range(1, NP):
            d = (p + j) % NP
            send(OS.at[i, d], OR.at[i, p], o_s.at[i], o_r.at[i], pdev(j))
        OR[i, p] = OS[i, p]

    offs = (0, -1, 1, -2, 2, -3, 3, 4)

    def stage_e(i):
        wait(OR.at[i, pl.ds(0, NP - 1)], o_r.at[i])
        if 0 < i < 7:
            send(OR.at[i], FN.at[z], f_s.at[i, 0], f_r.at[i, 0], zdev(offs[i]))
        if i == 7:
            H = NP // 2
            for k in range(2):
                send(OR.at[7, pl.ds(k * H, H)], RL.at[k], f_s.at[7, k], rl_r.at[k], zdev(1 - 2 * k))

    def relay(k):
        H = NP // 2
        s = 1 - 2 * k
        wait(RL.at[k], rl_r.at[k])
        send(RL.at[k], FN.at[zz(-s), pl.ds(k * H, H)], rl_s.at[k], f_r.at[7, k], zdev(3 * s))

    def combine(i):
        if i == 0:
            src, plane = OR.at[0], z
        else:
            plane = zz(-offs[i])
            src = FN.at[plane]
            if i < 7:
                wait(src, f_r.at[i, 0])
            else:
                for k in range(2):
                    wait(src.at[pl.ds(k * (NP // 2), NP // 2)], f_r.at[7, k])
        for b in range(T // TB):
            bb = slice(b * TB, (b + 1) * TB)
            cols = []
            for row in (TG[0:1, bb].astype(F32), TG[1:2, bb].astype(F32), rws[0:1, bb], rws[1:2, bb]):
                cols.append(jnp.transpose(jnp.broadcast_to(row, (128, TB))))
            mat = []
            for c in range(RP // 128):
                at = (lax.broadcasted_iota(I32, (TB, 128), 1) + (plane * RP + c * 128)).astype(F32)
                mat.append(jnp.where(at == cols[0], cols[2], 0.0) + jnp.where(at == cols[1], cols[3], 0.0))
            mat = jnp.concatenate(mat, axis=1).astype(BF16)

            def accumulate(n, carry):
                cc = pl.ds(pl.multiple_of(n * CB, CB), CB)
                got = jnp.dot(mat, src[:, :, cc].reshape(RP, CB), preferred_element_type=F32)
                if i == 0:
                    ACC[bb, cc] = got
                else:
                    ACC[bb, cc] = ACC[bb, cc] + got
                return carry

            lax.fori_loop(0, NB, accumulate, 0)

    stage_a(0)
    wait(WGU, w_sem.at[0])
    wait(WD, w_sem.at[1])
    stage_b(0)
    forward(0)
    stage_c(0)
    stage_d(0)
    forward(1)
    wait(TR.at[0], tg_r.at[0])
    stage_a(1)
    wait(TR.at[1], tg_r.at[1])
    stage_a(2)
    stage_e(0)
    stage_b(1)
    stage_b(2)
    stage_c(1)
    stage_c(2)
    stage_d(1)
    far(0)
    far(1)
    stage_a(3)
    stage_a(4)
    stage_d(2)
    stage_e(1)
    stage_b(3)
    stage_e(2)
    stage_b(4)
    stage_c(3)
    stage_c(4)
    stage_a(5)
    stage_a(6)
    stage_d(3)
    stage_d(4)
    stage_a(7)
    stage_b(5)
    stage_b(6)
    stage_e(3)
    stage_e(4)
    stage_c(5)
    stage_c(6)
    stage_b(7)
    stage_d(5)
    stage_d(6)
    stage_c(7)
    stage_e(5)
    stage_e(6)
    stage_d(7)
    combine(0)
    stage_e(7)
    combine(1)
    combine(2)
    relay(0)
    relay(1)
    for i in range(3, NZ):
        combine(i)

    squares(lambda b: ACC[b * TB:(b + 1) * TB, :], SQ2)
    share(SQ2, 1)
    wait(SQ2.at[pl.ds(0, NT - 1)], sq_r.at[1])
    for b in range(T // TB):
        sc = scales(SQ2, b)
        for c in range(W // 128):
            cc = slice(c * 128, (c + 1) * 128)
            out[b * TB:(b + 1) * TB, cc] = (ACC[b * TB:(b + 1) * TB, cc] * sc * fgain[0:1, cc]).astype(BF16)

    for k in range(2):
        wait(SQ.at[pl.ds(0, NT - 1)], sq_s.at[k])
        wait(RL.at[k], rl_s.at[k])
        wait(RL.at[k], f_s.at[7, k])
        wait(PR.at[k], ps_s.at[k, 0])
        wait(RL.at[k], ps_s.at[k, 1])
    wait(TR, tg_s)
    for k in range(4):
        for h in range(2):
            wait(DB.at[k, h], db_s.at[k, h])
    for i in range(NZ):
        wait(XR.at[i, pl.ds(0, NP - 1)], x_s.at[i])
        wait(GR.at[i, pl.ds(0, NT - 1)], g_s.at[i])
        wait(HB.at[i, pl.ds(0, NT - 1)], h_s.at[i])
        wait(OR.at[i, pl.ds(0, NP - 1)], o_s.at[i])
        if 0 < i < 7:
            wait(OR.at[i], f_s.at[i, 0])


def TR_CAP(rows, planar):
    return 4 * rows // (NZ * planar * 2)


def body(tokens, routes, route_weights, norm_gain, gate_weight, up_weight, down_weight, final_gain):
    NT = lax.axis_size("tp")
    NP = lax.axis_size("ep") // NZ
    T, W = tokens.shape
    FF = gate_weight.shape[2]
    FQ = FF // NT
    CAP = TR_CAP(T, NP)
    G2 = 2 * CAP
    M = NP * CAP
    rows = (NP, G2, W)
    vm = pltpu.VMEM
    dma = pltpu.SemaphoreType.DMA
    scratch = [
        vm((2, T // 2, W), BF16),
        vm((4, 2, T // 2, W), BF16),
        vm((8, T), I32),
        vm((4, 8, T), I32),
        vm((5, *rows), BF16),
        vm((NZ, *rows), BF16),
        vm((2, NP + NP // 2, G2, W), BF16),
        vm((3, *rows), BF16),
        vm((NZ, NT, 2, M, 2 * FQ), BF16),
        vm((NZ, NT, 2, M, 2 * FQ), BF16),
        vm((NZ, NT, 2, M, FQ), BF16),
        vm((NZ, *rows), BF16),
        vm((NZ, *rows), BF16),
        vm((NZ, *rows), BF16),
        vm((2, NP // 2, G2, W), BF16),
        vm((T, W), F32),
        vm((2, NT, W, 2 * FQ), BF16),
        vm((2, FF, W), BF16),
        vm((NT, 8, T), F32),
        vm((NT, 8, T), F32),
        dma((2,)),
        dma((2,)), dma((2,)),
        dma, dma((4,)),
        dma((4, 2)), dma((4, 2)),
        dma((2, 2)), dma((4,)),
        dma((NZ,)), dma((NZ,)),
        dma((NZ,)), dma((NZ,)),
        dma((NZ,)), dma((NZ,)),
        dma((NZ,)), dma((NZ,)),
        dma((NZ, 2)), dma((NZ, 2)),
        dma((2,)), dma((2,)),
    ]
    v = pl.BlockSpec(memory_space=pltpu.VMEM)
    a = pl.BlockSpec(memory_space=pl.ANY)
    return pl.pallas_call(
        functools.partial(layer_kernel, NP, NT),
        out_shape=jax.ShapeDtypeStruct((T, W), BF16),
        in_specs=[v, v, v, v, v, a, a, a],
        out_specs=v,
        scratch_shapes=scratch,
        compiler_params=pltpu.CompilerParams(
            collective_id=0, has_side_effects=True, vmem_limit_bytes=67043328
        ),
    )(
        tokens, routes.T, route_weights.T, norm_gain[None], final_gain[None],
        gate_weight, up_weight, down_weight,
    )


def solution(mesh):
    in_specs = (
        P("ep", "tp"),
        P("ep", None),
        P("ep", None),
        P("tp"),
        P("ep", "tp", None),
        P("ep", "tp", None),
        P("ep", None, "tp"),
        P("tp"),
    )
    out_specs = P("ep", "tp")
    return jax.shard_map(body, mesh=mesh, in_specs=in_specs, out_specs=out_specs, check_vma=False)
```

time: 368 us -> 227 us (0.62)
  Pallas kernels: 0 us -> 221 us
  waiting for transfers between devices: 159 us -> 0 us
  blocking collectives: 115 us -> 0 us
  starting transfers between devices: 33.5 us -> 0 us
  local copies, waits for them, and re-layouts: 34.4 us -> 2.26 us
  matrix products: 12.2 us -> 0 us
  other arithmetic: 11.5 us -> 0 us
    pallas_call x0 -> x1, Pallas kernels: none -> 221 us  [body(): pl.pallas_call(functools.partial(layer_kernel, NP, NT), out_shape=jax.Sha...]
    all_to_all x6 -> x0, waiting for transfers between devices: 159 us -> none  [the longest x1 94.9 us: serve_all(): lax.all_to_all(jnp.stack(results, axis=1), 'ep', split_axis=0, concat_axi...]
    all_to_all x2 -> x0, blocking collectives: 115 us -> none  [the longest x1 107 us: body(): lax.all_to_all(outgoing, 'ep', split_axis=0, concat_axis=0, tiled=True)]
    all_to_all x6 -> x0, starting transfers between devices: 33.5 us -> none  [the longest x3 12.4 us: from_everyone(): return lax.all_to_all(copies, axis, split_axis=0, concat_axis=0, tiled=True)]
    gather x3 -> x0, local copies, waits for them, and re-layouts: 20.6 us -> none  [the longest x2 10.9 us: body(): returned[position[:, which]].astype(jnp.float32)]
    dot_general x6 -> x0, matrix products: 12.2 us -> none  [the longest x2 5.27 us: expert_rows(): jnp.einsum('scf,fd->scd', hidden, w_down, preferred_element_type=jnp.floa...]
    reduce_sum x7 -> x0, other arithmetic: 4.89 us -> none  [the longest x2 2.33 us: sent_and_summed(): return jnp.sum(tiles.astype(jnp.float32), axis=0)]
    scatter x1 -> x0, local copies, waits for them, and re-layouts: 4.32 us -> none  [body(): jnp.full((experts * capacity,), tok_rows, jnp.int32).at[target].set(owners)]
  transfers between devices with their start and end apart: 6 -> 0, of which waited for: 5 -> 0; matrix products, arithmetic and copies ran while one was open for 5% -> 0% of each run, Pallas kernels for 0% -> 0%
where the time goes in v1:
time: 227 us; the launch traced here: 224 us
  Pallas kernels  221 us (97%)
    pallas_call x1, Pallas kernels, body(): pl.pallas_call(functools.partial(layer_kernel, NP, NT), out_shape=jax.Sha...  221 us

profile of v1, /device:TPU:36, one launch (start us, length us, event | category | flops | bytes accessed | tf_op | source)
XLA Modules:
  0.0 223.7 jit_solution(17705816814716903654)
XLA Ops:
  0.0 221.5 %shard_map.82 = bf16[512,1024]{1,0:T(8,128)(2,1)} custom-call(bf16[512,1024]{1,0:T(8,128)(2,1)} %tok.1, s32[2,512]{1,0:T(2,128)} %bitcast.4, f32[2,512]{1,0:T(2,128)} %bitcast.5, f32[1,1024]{1,0:T(1,128)} %bitcast.6, f32[1,1024]{1,0:T(1,128)} %bitcast.7, bf16[2,1024,512]{2,1,0:T(8,128)(2,1)} %gw.1, bf16[2,1024,512]{2,1,0:T(8,128)(2,1)} %uw.1, ...), custom_call_target="tpu_custom_call" | custom-call | tf_op jit(solution)/shard_map/pallas_call | solution.py:404
  221.5 2.3 %copy.10 = bf16[512,1024]{1,0:T(8,128)(2,1)} copy(bf16[512,1024]{1,0:T(8,128)(2,1)} %shard_map.82) | data formatting | bytes 2097152

commit v2 on v1

v2 whole, which is shorter than its diff:
```python
import functools

import jax
import jax.numpy as jnp
from jax import lax
from jax.experimental import pallas as pl
from jax.experimental.pallas import tpu as pltpu
from jax.sharding import PartitionSpec as P

EPSILON = 1e-06
NZ = 8
F32 = jnp.float32
BF16 = jnp.bfloat16
I32 = jnp.int32


def layer_kernel(
    NP, NT, tok, rts, rws, ngain, fgain, gw, uw, dw, out,
    DB, MT, MR, XS, XR, PS, GS, GR, HB, OS, OR, RV, CO, CM, RS, RD, ACC, WGU, WD, SQ, SQ2,
    w_sem, sq_s, sq_r, mt_s, mt_r, db_s, db_r, ps_s, x_s, x_r, g_s, g_r, h_s, h_r,
    o_s, o_r, rv_r, rd_s, rd_r,
):
    T, W = tok.shape
    HALF = T // 2
    CAP = cap_of(T, NP)
    G2 = 2 * CAP
    RP = NP * G2
    M = NP * CAP
    FQ = WGU.shape[3] // 2
    CB = RS.shape[3]
    NB = W // CB
    D = W * NT
    H = NP // 2
    NE = NZ * NP
    TB = min(128, T)
    ep = lax.axis_index("ep")
    y = lax.axis_index("tp")
    z = ep // NP
    p = ep % NP
    par = p % 2
    MESH = pl.DeviceIdType.MESH

    def zz(o):
        return (z + o + NZ) % NZ

    def at_plane(o, q):
        return {"ep": zz(o) * NP + q}

    def tdev(j):
        return {"tp": (y + j) % NT}

    def send(src, dst, ss, rs, dev):
        pltpu.make_async_remote_copy(
            src_ref=src, dst_ref=dst, send_sem=ss, recv_sem=rs, device_id=dev, device_id_type=MESH,
        ).start()

    def wait(ref, sem):
        pltpu.make_async_copy(ref, ref, sem).wait()

    barrier = pltpu.get_barrier_semaphore()

    def greet(j, carry):
        pl.semaphore_signal(barrier, inc=1, device_id={"ep": (ep + j) % NE}, device_id_type=MESH)
        return carry

    lax.fori_loop(1, NE, greet, 0)
    for j in range(1, NT):
        pl.semaphore_signal(barrier, inc=1, device_id=tdev(j), device_id_type=MESH)

    for m in range(2):
        for q in range(NT):
            cols = pl.ds(q * FQ, FQ)
            pltpu.make_async_copy(gw.at[m, :, cols], WGU.at[m, q, :, pl.ds(0, FQ)], w_sem.at[0]).start()
            pltpu.make_async_copy(uw.at[m, :, cols], WGU.at[m, q, :, pl.ds(FQ, FQ)], w_sem.at[0]).start()
    pltpu.make_async_copy(dw, WD, w_sem.at[1]).start()

    def squares(load, buf):
        for b in range(T // TB):
            v = load(b)
            s = jnp.sum(v * v, axis=1, keepdims=True)
            row = jnp.transpose(jnp.broadcast_to(s, (TB, 128)))
            buf[y, :, b * TB:(b + 1) * TB] = row[0:8, :]

    def share(buf, k):
        for j in range(1, NT):
            send(buf.at[y], buf.at[y], sq_s.at[k], sq_r.at[k], tdev(j))

    def scale_rows(buf):
        total = buf[0]
        for q in range(1, NT):
            total = total + buf[q]
        return lax.rsqrt(total / D + EPSILON)

    def send_h(h):
        part = tok.at[pl.ds(h * HALF, HALF)]
        send(part, DB.at[0, h], db_s.at[0, h], db_r.at[0, h], at_plane(1, p))
        send(part, DB.at[1, h], db_s.at[1, h], db_r.at[1, h], at_plane(-1, p))

    squares(lambda b: tok[b * TB:(b + 1) * TB, :].astype(F32), SQ)
    pl.semaphore_wait(barrier, NE - 1 + NT - 1)
    share(SQ, 0)
    send_h(0)

    r0 = rts[0:1, :]
    r1 = rts[1:2, :]
    eio = lax.broadcasted_iota(I32, (NE * 2, T), 0)
    oh0 = jnp.where(eio == r0, 1.0, 0.0)
    oh1 = jnp.where(eio == r1, 1.0, 0.0)
    up = jnp.where(
        lax.broadcasted_iota(I32, (T, T), 0) < lax.broadcasted_iota(I32, (T, T), 1), 1.0, 0.0
    ).astype(BF16)
    before = jnp.dot((oh0 + oh1).astype(BF16), up, preferred_element_type=F32)
    t0 = r0.astype(F32) * CAP + jnp.sum(oh0 * before, axis=0, keepdims=True)
    t1 = r1.astype(F32) * CAP + jnp.sum(oh1 * before, axis=0, keepdims=True)

    def near(k):
        wait(SQ.at[pl.ds(0, NT - 1)], sq_r.at[0])
        sub = lax.broadcasted_iota(I32, (8, T), 0)
        meta = jnp.where(sub == 0, t0, jnp.where(sub == 1, t1, scale_rows(SQ)))
        meta = jnp.where(sub == 2, rws[0:1, :], jnp.where(sub == 3, rws[1:2, :], meta))
        MT[...] = meta
        for slot, o in enumerate((1, -1, 2, -2)):
            send(MT, MR.at[slot], mt_s, mt_r.at[slot], at_plane(o, p))

    near(0)
    send_h(1)

    def pick(meta, at, xs, dst):
        rows = at.shape[0]
        s = meta[4:5, :]
        hit = (at == meta[0:1, :]) | (at == meta[1:2, :])
        scale = jnp.sum(jnp.where(hit, s, 0.0), axis=1, keepdims=True)
        sel = jnp.where(hit, 1.0, 0.0).astype(BF16)

        def cols(n, carry):
            cc = pl.ds(pl.multiple_of(n * CB, CB), CB)
            got = jnp.dot(sel[:, :HALF], xs[0][:, cc], preferred_element_type=F32)
            got = got + jnp.dot(sel[:, HALF:], xs[1][:, cc], preferred_element_type=F32)
            got = got * scale * ngain[0:1, cc]
            dst[:, :, cc] = got.astype(BF16).reshape(rows // G2, G2, CB)
            return carry

        lax.fori_loop(0, NB, cols, 0)

    def row_index(rows):
        return lax.broadcasted_iota(I32, (rows, T), 0)

    def stage_a(i):
        at = (row_index(RP) + z * RP).astype(F32)
        if i == 0:
            pick(MT, at, (tok.at[pl.ds(0, HALF)], tok.at[pl.ds(HALF, HALF)]), XS.at[0])
        else:
            wait_meta(i - 1)
            for h in range(2):
                wait_dense(i - 1, h)
            pick(MR.at[i - 1], at, (DB.at[i - 1, 0], DB.at[i - 1, 1]), XS.at[i])
        for j in range(1, NP):
            q = (p + j) % NP
            send(XS.at[i, q], XR.at[i, p], x_s.at[i], x_r.at[i], at_plane(0, q))
        XR[i, p] = XS[i, p]

    arrived = set()

    def wait_dense(k, h):
        if (k, h) not in arrived:
            arrived.add((k, h))
            wait(DB.at[k, h], db_r.at[k, h])

    def wait_meta(k):
        if k not in arrived:
            arrived.add(k)
            wait(MR.at[k], mt_r.at[k])

    def forward(h):
        for k in range(2):
            wait_dense(k, h)
            send(DB.at[k, h], DB.at[2 + k, h], db_s.at[2 + k, h], db_r.at[2 + k, h], at_plane(1 - 2 * k, p))

    def far(k):
        step = 1 - 2 * k
        for h in range(2):
            wait_dense(2 + k, h)
        wait_meta(2 + k)
        xs = (DB.at[2 + k, 0], DB.at[2 + k, 1])
        pick(MR.at[2 + k], (row_index(RP) + zz(step) * RP).astype(F32), xs, PS.at[k, pl.ds(0, NP)])
        for j in range(NP):
            q = (p + j) % NP
            send(PS.at[k, q], XR.at[5 + k, p], ps_s.at[k, 0], x_r.at[5 + k], at_plane(step, q))
        it = row_index(RP // 2)
        at = it // G2 * (2 * G2) + it % G2 + (zz(2 * step) * RP + k * G2)
        pick(MR.at[2 + k], at.astype(F32), xs, PS.at[k, pl.ds(NP, H)])
        for j in range(H):
            q = (p // 2 + j) % H
            send(PS.at[k, NP + q], XR.at[7, p], ps_s.at[k, 1], x_r.at[7], at_plane(2 * step, 2 * q + k))

    def stage_b(i):
        wait(XR.at[i, pl.ds(0, NP - 1)] if i <= 4 else XR.at[i], x_r.at[i])

        def one(j, carry):
            q = (y + 1 + j) % NT
            for m in range(2):
                rows = XR[i, :, m * CAP:(m + 1) * CAP, :].reshape(M, W)
                got = jnp.dot(rows, WGU[m, q], preferred_element_type=F32)
                GS[i, q, m] = got.astype(BF16)

            @pl.when(j < NT - 1)
            def _():
                send(GS.at[i, q], GR.at[i, y], g_s.at[i], g_r.at[i], {"tp": q})

            return carry

        lax.fori_loop(0, NT, one, 0)

    def stage_c(i):
        wait(GR.at[i, pl.ds(0, NT - 1)], g_r.at[i])
        for m in range(2):
            total = GS[i, y, m].astype(F32)
            for j in range(1, NT):
                total = total + GR[i, (y + j) % NT, m].astype(F32)
            gate = total[:, :FQ]
            HB[i, y, m] = (gate / (1.0 + jnp.exp(-gate)) * total[:, FQ:]).astype(BF16)
        for j in range(1, NT):
            send(HB.at[i, y], HB.at[i, y], h_s.at[i], h_r.at[i], tdev(j))

    def stage_d(i):
        wait(HB.at[i, pl.ds(0, NT - 1)], h_r.at[i])
        for m in range(2):
            hid = jnp.concatenate([HB[i, q, m] for q in range(NT)], axis=1)

            def cols(n, carry):
                cc = pl.ds(pl.multiple_of(n * CB, CB), CB)
                got = jnp.dot(hid, WD[m, :, cc], preferred_element_type=F32)
                OS[i, :, m * CAP:(m + 1) * CAP, cc] = got.astype(BF16).reshape(NP, CAP, CB)
                return carry

            lax.fori_loop(0, NB, cols, 0)
        if i == 0:
            for j in range(1, NP):
                q = (p + j) % NP
                send(OS.at[0, q], OR.at[p], o_s.at[0], o_r, at_plane(0, q))
            OR[p] = OS[0, p]
        elif i < 7:
            d = (i + 1) // 2
            side = (i + 1) % 2
            for j in range(1 if d == 1 else 0, NP):
                q = (p + j) % NP
                hop = (d - 1) * (2 * side - 1)
                send(OS.at[i, q], RV.at[side, (d - 1) * NP + p], o_s.at[i], rv_r.at[side, d - 1], at_plane(hop, q))
            if d == 1:
                RV[side, p] = OS[i, p]
        else:
            side = 1 - par
            for j in range(NP):
                q = (p + j) % NP
                send(OS.at[7, q], RV.at[side, 3 * NP + p // 2], o_s.at[7], rv_r.at[side, 3], at_plane(3 - 6 * par, q))

    def matrix(meta, at, b):
        bb = slice(b * TB, (b + 1) * TB)
        cols = [jnp.transpose(jnp.broadcast_to(meta[r:r + 1, bb], (128, TB))) for r in range(4)]
        out = []
        for a in at:
            out.append(jnp.where(a == cols[0], cols[2], 0.0) + jnp.where(a == cols[1], cols[3], 0.0))
        return jnp.concatenate(out, axis=1).astype(BF16)

    def lanes(base):
        return lax.broadcasted_iota(I32, (TB, 128), 1) + base

    def mats(k):
        own = [lanes(z * RP + c * 128).astype(F32) for c in range(RP // 128)]
        for b in range(T // TB):
            CO[b * TB:(b + 1) * TB, :] = matrix(MT, own, b)
        for side in range(2):
            wait_meta(side)
            s = 1 - 2 * side
            at = [lanes(zz(s * d) * RP + c * 128) for d in range(3) for c in range(RP // 128)]
            for c in range(RP // 256):
                it = lanes(c * 128)
                at.append(it // G2 * (2 * G2) + it % G2 + (zz(3 * s) * RP + (1 - side) * G2))
            at = [a.astype(F32) for a in at]
            for b in range(T // TB):
                CM[side, b * TB:(b + 1) * TB, :] = matrix(MR.at[side], at, b)

    def own_part(k):
        wait(OR.at[pl.ds(0, NP - 1)], o_r)

        def cols(n, carry):
            cc = pl.ds(pl.multiple_of(n * CB, CB), CB)
            ACC[n] = jnp.dot(CO[...], OR[:, :, cc].reshape(RP, CB), preferred_element_type=F32)
            return carry

        lax.fori_loop(0, NB, cols, 0)

    def relay(side):
        wait(RV.at[side, pl.ds(0, NP - 1)], rv_r.at[side, 0])
        for d in range(1, 3):
            wait(RV.at[side, pl.ds(d * NP, NP)], rv_r.at[side, d])
        wait(RV.at[side, pl.ds(3 * NP, H)], rv_r.at[side, 3])

        def cols(n, carry):
            cc = pl.ds(pl.multiple_of(n * CB, CB), CB)
            rows = RV[side, :, :, cc].reshape(CM.shape[2], CB)
            got = jnp.dot(CM[side], rows, preferred_element_type=F32)
            RS[side, n] = got.astype(BF16)
            send(RS.at[side, n], RD.at[side, n], rd_s.at[side, n], rd_r.at[side, n], at_plane(2 * side - 1, p))
            return carry

        lax.fori_loop(0, NB, cols, 0)

    stage_a(0)
    forward(0)
    wait(WGU, w_sem.at[0])
    wait(WD, w_sem.at[1])
    stage_b(0)
    stage_c(0)
    forward(1)
    stage_a(2)
    mats(0)
    stage_d(0)
    stage_a(1)
    stage_b(2)
    own_part(0)
    stage_c(2)
    stage_b(1)
    far(1)
    far(0)
    stage_d(2)
    stage_c(1)
    stage_a(3)
    stage_a(4)
    stage_d(1)
    stage_b(6)
    stage_b(5)
    stage_c(6)
    stage_c(5)
    stage_b(7)
    stage_b(3)
    stage_d(6)
    stage_d(5)
    stage_b(4)
    stage_c(7)
    stage_c(3)
    stage_c(4)
    stage_d(7)
    stage_d(3)
    stage_d(4)
    relay(1)
    relay(0)

    def finish(n, carry):
        for side in range(2):
            wait(RD.at[side, n], rd_r.at[side, n])
        ACC[n] = ACC[n] + RD[0, n].astype(F32) + RD[1, n].astype(F32)
        return carry

    lax.fori_loop(0, NB, finish, 0)

    def block(b):
        return jnp.concatenate([ACC[n, b * TB:(b + 1) * TB, :] for n in range(NB)], axis=1)

    squares(block, SQ2)
    share(SQ2, 1)
    wait(SQ2.at[pl.ds(0, NT - 1)], sq_r.at[1])
    final = scale_rows(SQ2)
    for b in range(T // TB):
        sc = jnp.transpose(jnp.broadcast_to(final[0:1, b * TB:(b + 1) * TB], (128, TB)))
        for c in range(W // 128):
            n, l = c * 128 // CB, c * 128 % CB
            v = ACC[n, b * TB:(b + 1) * TB, l:l + 128] * sc * fgain[0:1, c * 128:(c + 1) * 128]
            out[b * TB:(b + 1) * TB, c * 128:(c + 1) * 128] = v.astype(BF16)

    for k in range(2):
        wait(SQ.at[pl.ds(0, NT - 1)], sq_s.at[k])
        wait(PS.at[k, pl.ds(0, NP)], ps_s.at[k, 0])
        wait(PS.at[k, pl.ds(NP, H)], ps_s.at[k, 1])
        for n in range(NB):
            wait(RD.at[k, n], rd_s.at[k, n])
    wait(MR, mt_s)
    for k in range(4):
        for h in range(2):
            wait(DB.at[k, h], db_s.at[k, h])
    for i in range(NZ):
        if i <= 4:
            wait(XR.at[i, pl.ds(0, NP - 1)], x_s.at[i])
        wait(GR.at[i, pl.ds(0, NT - 1)], g_s.at[i])
        wait(HB.at[i, pl.ds(0, NT - 1)], h_s.at[i])
        wait(OS.at[i, pl.ds(0, NP - 1)] if i <= 2 else OS.at[i], o_s.at[i])


def cap_of(rows, planar):
    return 4 * rows // (NZ * planar * 2)


def body(tokens, routes, route_weights, norm_gain, gate_weight, up_weight, down_weight, final_gain):
    NT = lax.axis_size("tp")
    NP = lax.axis_size("ep") // NZ
    T, W = tokens.shape
    FF = gate_weight.shape[2]
    FQ = FF // NT
    CAP = cap_of(T, NP)
    G2 = 2 * CAP
    RP = NP * G2
    M = NP * CAP
    CB = 256 if W % 256 == 0 else 128
    NB = W // CB
    rows = (NP, G2, W)
    vm = pltpu.VMEM
    dma = pltpu.SemaphoreType.DMA
    scratch = [
        vm((4, 2, T // 2, W), BF16),
        vm((8, T), F32),
        vm((4, 8, T), F32),
        vm((5, *rows), BF16),
        vm((NZ, *rows), BF16),
        vm((2, NP + NP // 2, G2, W), BF16),
        vm((NZ, NT, 2, M, 2 * FQ), BF16),
        vm((NZ, NT, 2, M, 2 * FQ), BF16),
        vm((NZ, NT, 2, M, FQ), BF16),
        vm((NZ, *rows), BF16),
        vm(rows, BF16),
        vm((2, 3 * NP + NP // 2, G2, W), BF16),
        vm((T, RP), BF16),
        vm((2, T, 3 * RP + RP // 2), BF16),
        vm((2, NB, T, CB), BF16),
        vm((2, NB, T, CB), BF16),
        vm((NB, T, CB), F32),
        vm((2, NT, W, 2 * FQ), BF16),
        vm((2, FF, W), BF16),
        vm((NT, 8, T), F32),
        vm((NT, 8, T), F32),
        dma((2,)),
        dma((2,)), dma((2,)),
        dma, dma((4,)),
        dma((4, 2)), dma((4, 2)),
        dma((2, 2)),
        dma((5,)), dma((NZ,)),
        dma((NZ,)), dma((NZ,)),
        dma((NZ,)), dma((NZ,)),
        dma((NZ,)), dma,
        dma((2, 4)),
        dma((2, NB)), dma((2, NB)),
    ]
    v = pl.BlockSpec(memory_space=pltpu.VMEM)
    a = pl.BlockSpec(memory_space=pl.ANY)
    return pl.pallas_call(
        functools.partial(layer_kernel, NP, NT),
        out_shape=jax.ShapeDtypeStruct((T, W), BF16),
        in_specs=[v, v, v, v, v, a, a, a],
        out_specs=v,
        scratch_shapes=scratch,
        compiler_params=pltpu.CompilerParams(
            collective_id=0, has_side_effects=True, vmem_limit_bytes=67043328
        ),
    )(
        tokens, routes.T, route_weights.T, norm_gain[None], final_gain[None],
        gate_weight, up_weight, down_weight,
    )


def solution(mesh):
    in_specs = (
        P("ep", "tp"),
        P("ep", None),
        P("ep", None),
        P("tp"),
        P("ep", "tp", None),
        P("ep", "tp", None),
        P("ep", None, "tp"),
        P("tp"),
    )
    out_specs = P("ep", "tp")
    return jax.shard_map(body, mesh=mesh, in_specs=in_specs, out_specs=out_specs, check_vma=False)
```

time: 227 us -> 195 us (0.86); the launches traced: 224 us -> 195 us
  Pallas kernels: 221 us -> 193 us
    pallas_call x1, Pallas kernels: 221 us -> 193 us  [body(): pl.pallas_call(functools.partial(layer_kernel, NP, NT), out_shape=jax.Sha...]
where the time goes in v2:
time: 195 us
  Pallas kernels  193 us (99%)
  local copies, waits for them, and re-layouts  2.26 us (1%)
    pallas_call x1, Pallas kernels, body(): pl.pallas_call(functools.partial(layer_kernel, NP, NT), out_shape=jax.Sha...  193 us

profile of v2, /device:TPU:36, one launch (start us, length us, event | category | flops | bytes accessed | tf_op | source)
XLA Modules:
  0.0 194.9 jit_solution(11906226812421430523)
XLA Ops:
  0.0 192.7 %shard_map.82 = bf16[512,1024]{1,0:T(8,128)(2,1)} custom-call(bf16[512,1024]{1,0:T(8,128)(2,1)} %tok.1, s32[2,512]{1,0:T(2,128)} %bitcast.4, f32[2,512]{1,0:T(2,128)} %bitcast.5, f32[1,1024]{1,0:T(1,128)} %bitcast.6, f32[1,1024]{1,0:T(1,128)} %bitcast.7, bf16[2,1024,512]{2,1,0:T(8,128)(2,1)} %gw.1, bf16[2,1024,512]{2,1,0:T(8,128)(2,1)} %uw.1, ...), custom_call_target="tpu_custom_call" | custom-call | tf_op jit(solution)/shard_map/pallas_call | solution.py:444
  192.7 2.3 %copy.10 = bf16[512,1024]{1,0:T(8,128)(2,1)} copy(bf16[512,1024]{1,0:T(8,128)(2,1)} %shard_map.82) | data formatting | bytes 2097152

commit v3 on v2

v3 whole, which is shorter than its diff:
```python
import functools

import jax
import jax.numpy as jnp
from jax import lax
from jax.experimental import pallas as pl
from jax.experimental.pallas import tpu as pltpu
from jax.sharding import PartitionSpec as P

EPSILON = 1e-06
NZ = 8
F32 = jnp.float32
BF16 = jnp.bfloat16
I32 = jnp.int32


def layer_kernel(
    NP, NT, tok, rts, rws, ngain, fgain, gw, uw, dw, out,
    DB, MT, MR, XS, XR, PS, GS, GR, HB, OS, OR, RV, RW, CO, CM, RS, RD, ACC, WGU, WD, SQ, SQ2, OUT,
    w_sem, sq_s, sq_r, mt_s, mt_r, db_s, db_r, ps_s, x_s, x_r, g_s, g_r, h_s, h_r,
    o_s, o_r, rv_r, rd_s, rd_r, out_s,
):
    T, W = tok.shape
    HALF = T // 2
    CAP = cap_of(T, NP)
    G2 = 2 * CAP
    RP = NP * G2
    M = NP * CAP
    FQ = WGU.shape[3] // 2
    CB = RS.shape[3]
    KA = 6 * NP * CAP
    NB = W // CB
    D = W * NT
    H = NP // 2
    NE = NZ * NP
    TB = min(128, T)
    ep = lax.axis_index("ep")
    y = lax.axis_index("tp")
    z = ep // NP
    p = ep % NP
    par = p % 2
    MESH = pl.DeviceIdType.MESH

    def zz(o):
        return (z + o + NZ) % NZ

    def at_plane(o, q):
        return {"ep": zz(o) * NP + q}

    def tdev(j):
        return {"tp": (y + j) % NT}

    def send(src, dst, ss, rs, dev):
        pltpu.make_async_remote_copy(
            src_ref=src, dst_ref=dst, send_sem=ss, recv_sem=rs, device_id=dev, device_id_type=MESH,
        ).start()

    def wait(ref, sem):
        pltpu.make_async_copy(ref, ref, sem).wait()

    barrier = pltpu.get_barrier_semaphore()

    def greet(j, carry):
        for o in (-3, -2, -1, 1, 2, 3):
            pl.semaphore_signal(barrier, inc=1, device_id=at_plane(o, j), device_id_type=MESH)
        return carry

    lax.fori_loop(0, NP, greet, 0)
    for j in range(1, NP):
        pl.semaphore_signal(barrier, inc=1, device_id=at_plane(0, (p + j) % NP), device_id_type=MESH)
    for j in range(1, NT):
        pl.semaphore_signal(barrier, inc=1, device_id=tdev(j), device_id_type=MESH)

    for m in range(2):
        for q in range(NT):
            cols = pl.ds(q * FQ, FQ)
            pltpu.make_async_copy(gw.at[m, :, cols], WGU.at[m, q, :, pl.ds(0, FQ)], w_sem.at[0]).start()
            pltpu.make_async_copy(uw.at[m, :, cols], WGU.at[m, q, :, pl.ds(FQ, FQ)], w_sem.at[0]).start()
    pltpu.make_async_copy(dw, WD, w_sem.at[1]).start()

    def squares(load, buf):
        for b in range(T // TB):
            v = load(b)
            s = jnp.sum(v * v, axis=1, keepdims=True)
            row = jnp.transpose(jnp.broadcast_to(s, (TB, 128)))
            buf[y, :, b * TB:(b + 1) * TB] = row[0:8, :]

    def share(buf, k):
        for j in range(1, NT):
            send(buf.at[y], buf.at[y], sq_s.at[k], sq_r.at[k], tdev(j))

    def scale_rows(buf):
        total = buf[0]
        for q in range(1, NT):
            total = total + buf[q]
        return lax.rsqrt(total / D + EPSILON)

    def send_h(h):
        part = tok.at[pl.ds(h * HALF, HALF)]
        send(part, DB.at[0, h], db_s.at[0, h], db_r.at[0, h], at_plane(1, p))
        send(part, DB.at[1, h], db_s.at[1, h], db_r.at[1, h], at_plane(-1, p))

    squares(lambda b: tok[b * TB:(b + 1) * TB, :].astype(F32), SQ)
    pl.semaphore_wait(barrier, 7 * NP - 1 + NT - 1)
    share(SQ, 0)
    send_h(0)

    r0 = rts[0:1, :]
    r1 = rts[1:2, :]
    eio = lax.broadcasted_iota(I32, (NE * 2, T), 0)
    oh0 = jnp.where(eio == r0, 1.0, 0.0)
    oh1 = jnp.where(eio == r1, 1.0, 0.0)
    up = jnp.where(
        lax.broadcasted_iota(I32, (T, T), 0) < lax.broadcasted_iota(I32, (T, T), 1), 1.0, 0.0
    ).astype(BF16)
    before = jnp.dot((oh0 + oh1).astype(BF16), up, preferred_element_type=F32)
    t0 = r0.astype(F32) * CAP + jnp.sum(oh0 * before, axis=0, keepdims=True)
    t1 = r1.astype(F32) * CAP + jnp.sum(oh1 * before, axis=0, keepdims=True)

    def near(k):
        wait(SQ.at[pl.ds(0, NT - 1)], sq_r.at[0])
        sub = lax.broadcasted_iota(I32, (8, T), 0)
        meta = jnp.where(sub == 0, t0, jnp.where(sub == 1, t1, scale_rows(SQ)))
        meta = jnp.where(sub == 2, rws[0:1, :], jnp.where(sub == 3, rws[1:2, :], meta))
        MT[...] = meta
        for slot, o in enumerate((1, -1, 2, -2)):
            send(MT, MR.at[slot], mt_s, mt_r.at[slot], at_plane(o, p))

    near(0)
    send_h(1)

    def pick(meta, at, xs, dst):
        rows = at.shape[0]
        s = meta[4:5, :]
        hit = (at == meta[0:1, :]) | (at == meta[1:2, :])
        scale = jnp.sum(jnp.where(hit, s, 0.0), axis=1, keepdims=True)
        sel = jnp.where(hit, 1.0, 0.0).astype(BF16)

        def cols(n, carry):
            cc = pl.ds(pl.multiple_of(n * CB, CB), CB)
            got = jnp.dot(sel[:, :HALF], xs[0][:, cc], preferred_element_type=F32)
            got = got + jnp.dot(sel[:, HALF:], xs[1][:, cc], preferred_element_type=F32)
            got = got * scale * ngain[0:1, cc]
            dst[:, :, :, cc] = got.astype(BF16).reshape(2, rows // G2, CAP, CB)
            return carry

        lax.fori_loop(0, NB, cols, 0)

    def row_index(rows, spread=1):
        r = lax.broadcasted_iota(I32, (rows, T), 0)
        half = rows // 2
        return (r % half) // CAP * (G2 * spread) + r // half * CAP + r % CAP

    def stage_a(i):
        at = (row_index(RP) + z * RP).astype(F32)
        if i == 0:
            pick(MT, at, (tok.at[pl.ds(0, HALF)], tok.at[pl.ds(HALF, HALF)]), XS.at[0])
        else:
            wait_meta(i - 1)
            for h in range(2):
                wait_dense(i - 1, h)
            pick(MR.at[i - 1], at, (DB.at[i - 1, 0], DB.at[i - 1, 1]), XS.at[i])
        for m in range(2):
            for j in range(1, NP):
                q = (p + j) % NP
                send(XS.at[i, m, q], XR.at[i, m, p], x_s.at[i, m], x_r.at[i, m], at_plane(0, q))
        for m in range(2):
            XR[i, m, p] = XS[i, m, p]

    arrived = set()

    def wait_dense(k, h):
        if (k, h) not in arrived:
            arrived.add((k, h))
            wait(DB.at[k, h], db_r.at[k, h])

    def wait_meta(k):
        if k not in arrived:
            arrived.add(k)
            wait(MR.at[k], mt_r.at[k])

    def forward(h):
        for k in range(2):
            wait_dense(k, h)
            send(DB.at[k, h], DB.at[2 + k, h], db_s.at[2 + k, h], db_r.at[2 + k, h], at_plane(1 - 2 * k, p))

    def far3(k):
        step = 1 - 2 * k
        for h in range(2):
            wait_dense(2 + k, h)
        wait_meta(2 + k)
        xs = (DB.at[2 + k, 0], DB.at[2 + k, 1])
        pick(MR.at[2 + k], (row_index(RP) + zz(step) * RP).astype(F32), xs, PS.at[k, :, pl.ds(0, NP)])
        for m in range(2):
            for j in range(NP):
                q = (p + j) % NP
                send(PS.at[k, m, q], XR.at[5 + k, m, p], ps_s.at[k, 0, m], x_r.at[5 + k, m], at_plane(step, q))

    def far4(k):
        step = 1 - 2 * k
        xs = (DB.at[2 + k, 0], DB.at[2 + k, 1])
        at = row_index(RP // 2, 2) + (zz(2 * step) * RP + k * G2)
        pick(MR.at[2 + k], at.astype(F32), xs, PS.at[k, :, pl.ds(NP, H)])
        for m in range(2):
            for j in range(H):
                q = (p // 2 + j) % H
                send(PS.at[k, m, NP + q], XR.at[7, m, p], ps_s.at[k, 1, m], x_r.at[7, m], at_plane(2 * step, 2 * q + k))

    def stage_b(i, m):
        wait(XR.at[i, m, pl.ds(0, NP - 1)] if i <= 4 else XR.at[i, m], x_r.at[i, m])

        def one(j, carry):
            q = (y + 1 + j) % NT
            rows = XR[i, m].reshape(M, W)
            got = jnp.dot(rows, WGU[m, q], preferred_element_type=F32)
            GS[i, m, q] = got.astype(BF16)

            @pl.when(j < NT - 1)
            def _():
                send(GS.at[i, m, q], GR.at[i, m, y], g_s.at[i, m], g_r.at[i, m], {"tp": q})

            return carry

        lax.fori_loop(0, NT, one, 0)

    def stage_c(i, m):
        wait(GR.at[i, m, pl.ds(0, NT - 1)], g_r.at[i, m])
        total = GS[i, m, y].astype(F32)
        for j in range(1, NT):
            total = total + GR[i, m, (y + j) % NT].astype(F32)
        gate = total[:, :FQ]
        HB[i, m, y] = (gate / (1.0 + jnp.exp(-gate)) * total[:, FQ:]).astype(BF16)
        for j in range(1, NT):
            send(HB.at[i, m, y], HB.at[i, m, y], h_s.at[i, m], h_r.at[i, m], tdev(j))

    def stage_d(i, m):
        wait(HB.at[i, m, pl.ds(0, NT - 1)], h_r.at[i, m])
        hid = jnp.concatenate([HB[i, m, q] for q in range(NT)], axis=1)

        def cols(n, carry):
            cc = pl.ds(pl.multiple_of(n * CB, CB), CB)
            got = jnp.dot(hid, WD[m, :, cc], preferred_element_type=F32)
            OS[i, m, :, :, cc] = got.astype(BF16).reshape(NP, CAP, CB)
            return carry

        lax.fori_loop(0, NB, cols, 0)
        if i == 0:
            for j in range(1, NP):
                q = (p + j) % NP
                send(OS.at[0, m, q], OR.at[m, p], o_s.at[0, m], o_r.at[m], at_plane(0, q))
            OR[m, p] = OS[0, m, p]
        elif i < 7:
            d = (i + 1) // 2
            side = (i + 1) % 2
            for j in range(1 if d == 1 else 0, NP):
                q = (p + j) % NP
                hop = (d - 1) * (2 * side - 1)
                send(
                    OS.at[i, m, q], RV.at[side, m, (d - 1) * NP + p], o_s.at[i, m],
                    rv_r.at[side, d - 1, m], at_plane(hop, q),
                )
            if d == 1:
                RV[side, m, p] = OS[i, m, p]
        else:
            side = 1 - par
            for j in range(NP):
                q = (p + j) % NP
                send(
                    OS.at[7, m, q], RW.at[side, m, p // 2], o_s.at[7, m],
                    rv_r.at[side, 3, m], at_plane(3 - 6 * par, q),
                )

    def matrix(meta, at, b):
        bb = slice(b * TB, (b + 1) * TB)
        cols = [jnp.transpose(jnp.broadcast_to(meta[r:r + 1, bb], (128, TB))) for r in range(4)]
        out = []
        for a in at:
            out.append(jnp.where(a == cols[0], cols[2], 0.0) + jnp.where(a == cols[1], cols[3], 0.0))
        return jnp.concatenate(out, axis=1).astype(BF16)

    def lanes(base):
        return lax.broadcasted_iota(I32, (TB, 128), 1) + base

    def mats(k):
        def place(col, groups, step):
            m = col // (groups * CAP)
            r = col % (groups * CAP)
            return r // CAP % NP * (G2 * step) + m * CAP + r % CAP

        own = [(z * RP + place(lanes(c * 128), NP, 1)).astype(F32) for c in range(RP // 128)]
        for b in range(T // TB):
            CO[b * TB:(b + 1) * TB, :] = matrix(MT, own, b)
        for side in range(2):
            wait_meta(side)
            s = 1 - 2 * side
            at = []
            for c in range(KA // 128):
                col = lanes(c * 128)
                d = col % (KA // 2) // (NP * CAP)
                plane = jnp.where(d == 0, z, jnp.where(d == 1, zz(s), zz(2 * s)))
                at.append((plane * RP + place(col, 3 * NP, 1)).astype(F32))
            for c in range(RP // 256):
                col = place(lanes(c * 128), H, 2)
                at.append((col + (zz(3 * s) * RP + (1 - side) * G2)).astype(F32))
            for b in range(T // TB):
                CM[side, b * TB:(b + 1) * TB, :] = matrix(MR.at[side], at, b)

    def own_part(k):
        for m in range(2):
            wait(OR.at[m, pl.ds(0, NP - 1)], o_r.at[m])

        def cols(n, carry):
            cc = pl.ds(pl.multiple_of(n * CB, CB), CB)
            ACC[n] = jnp.dot(CO[...], OR[:, :, :, cc].reshape(RP, CB), preferred_element_type=F32)
            return carry

        lax.fori_loop(0, NB, cols, 0)

    def relay(k):
        for m in range(2):
            for side in range(2):
                wait(RV.at[side, m, pl.ds(0, NP - 1)], rv_r.at[side, 0, m])
                for d in range(1, 3):
                    wait(RV.at[side, m, pl.ds(d * NP, NP)], rv_r.at[side, d, m])
                wait(RW.at[side, m], rv_r.at[side, 3, m])

        def cols(n, carry):
            cc = pl.ds(pl.multiple_of(n * CB, CB), CB)
            for side in range(2):
                rows = RV[side, :, :, :, cc].reshape(KA, CB)
                more = RW[side, :, :, :, cc].reshape(RP // 2, CB)
                got = jnp.dot(CM[side, :, :KA], rows, preferred_element_type=F32)
                got = got + jnp.dot(CM[side, :, KA:], more, preferred_element_type=F32)
                RS[side, n] = got.astype(BF16)
                send(RS.at[side, n], RD.at[side, n], rd_s.at[side, n], rd_r.at[side, n], at_plane(2 * side - 1, p))
            return carry

        lax.fori_loop(0, NB, cols, 0)

    stage_a(0)
    wait(WGU, w_sem.at[0])
    stage_b(0, 0)
    stage_b(0, 1)
    forward(0)
    stage_c(0, 0)
    stage_c(0, 1)
    wait(WD, w_sem.at[1])
    stage_d(0, 0)
    stage_a(2)
    forward(1)
    stage_b(2, 0)
    stage_a(1)
    stage_b(2, 1)
    stage_d(0, 1)
    stage_c(2, 1)
    stage_b(1, 1)
    stage_b(1, 0)
    stage_c(2, 0)
    far3(0)
    far3(1)
    stage_a(3)
    far4(1)
    stage_c(1, 1)
    stage_c(1, 0)
    far4(0)
    stage_a(4)
    stage_b(5, 0)
    stage_d(1, 0)
    stage_b(6, 0)
    stage_d(1, 1)
    stage_d(2, 1)
    stage_c(5, 0)
    stage_c(6, 0)
    stage_b(6, 1)
    stage_b(5, 1)
    stage_d(2, 0)
    stage_b(3, 0)
    stage_d(5, 0)
    stage_d(6, 0)
    stage_c(6, 1)
    stage_c(5, 1)
    stage_b(7, 0)
    stage_c(3, 0)
    stage_b(3, 1)
    stage_b(7, 1)
    stage_d(6, 1)
    stage_d(5, 1)
    mats(0)
    own_part(0)
    stage_c(7, 0)
    stage_b(4, 0)
    stage_c(3, 1)
    stage_c(7, 1)
    stage_b(4, 1)
    stage_d(7, 0)
    stage_d(3, 1)
    stage_c(4, 0)
    stage_d(7, 1)
    stage_c(4, 1)
    stage_d(4, 1)
    stage_d(4, 0)
    stage_d(3, 0)
    relay(0)

    def finish(n, carry):
        for side in range(2):
            wait(RD.at[side, n], rd_r.at[side, n])
        ACC[n] = ACC[n] + RD[0, n].astype(F32) + RD[1, n].astype(F32)
        return carry

    lax.fori_loop(0, NB, finish, 0)

    def block(b):
        return jnp.concatenate([ACC[n, b * TB:(b + 1) * TB, :] for n in range(NB)], axis=1)

    squares(block, SQ2)
    share(SQ2, 1)
    wait(SQ2.at[pl.ds(0, NT - 1)], sq_r.at[1])
    final = scale_rows(SQ2)
    for b in range(T // TB):
        sc = jnp.transpose(jnp.broadcast_to(final[0:1, b * TB:(b + 1) * TB], (128, TB)))
        for c in range(W // 128):
            n, l = c * 128 // CB, c * 128 % CB
            v = ACC[n, b * TB:(b + 1) * TB, l:l + 128] * sc * fgain[0:1, c * 128:(c + 1) * 128]
            OUT[b * TB:(b + 1) * TB, c * 128:(c + 1) * 128] = v.astype(BF16)
        pltpu.make_async_copy(OUT.at[pl.ds(b * TB, TB)], out.at[pl.ds(b * TB, TB)], out_s).start()

    for k in range(2):
        wait(SQ.at[pl.ds(0, NT - 1)], sq_s.at[k])
        for m in range(2):
            wait(PS.at[k, m, pl.ds(0, NP)], ps_s.at[k, 0, m])
            wait(PS.at[k, m, pl.ds(NP, H)], ps_s.at[k, 1, m])
        for n in range(NB):
            wait(RD.at[k, n], rd_s.at[k, n])
    wait(MR, mt_s)
    for k in range(4):
        for h in range(2):
            wait(DB.at[k, h], db_s.at[k, h])
    for i in range(NZ):
        for m in range(2):
            if i <= 4:
                wait(XR.at[i, m, pl.ds(0, NP - 1)], x_s.at[i, m])
            wait(GR.at[i, m, pl.ds(0, NT - 1)], g_s.at[i, m])
            wait(HB.at[i, m, pl.ds(0, NT - 1)], h_s.at[i, m])
            wait(OS.at[i, m, pl.ds(0, NP - 1)] if i <= 2 else OS.at[i, m], o_s.at[i, m])
    wait(OUT, out_s)


def cap_of(rows, planar):
    return 4 * rows // (NZ * planar * 2)


def body(tokens, routes, route_weights, norm_gain, gate_weight, up_weight, down_weight, final_gain):
    NT = lax.axis_size("tp")
    NP = lax.axis_size("ep") // NZ
    T, W = tokens.shape
    FF = gate_weight.shape[2]
    FQ = FF // NT
    CAP = cap_of(T, NP)
    G2 = 2 * CAP
    RP = NP * G2
    M = NP * CAP
    CB = 256 if W % 256 == 0 else 128
    NB = W // CB
    rows = (2, NP, CAP, W)
    vm = pltpu.VMEM
    dma = pltpu.SemaphoreType.DMA
    scratch = [
        vm((4, 2, T // 2, W), BF16),
        vm((8, T), F32),
        vm((4, 8, T), F32),
        vm((5, *rows), BF16),
        vm((NZ, *rows), BF16),
        vm((2, 2, NP + NP // 2, CAP, W), BF16),
        vm((NZ, 2, NT, M, 2 * FQ), BF16),
        vm((NZ, 2, NT, M, 2 * FQ), BF16),
        vm((NZ, 2, NT, M, FQ), BF16),
        vm((NZ, *rows), BF16),
        vm(rows, BF16),
        vm((2, 2, 3 * NP, CAP, W), BF16),
        vm((2, 2, NP // 2, CAP, W), BF16),
        vm((T, RP), BF16),
        vm((2, T, 3 * RP + RP // 2), BF16),
        vm((2, NB, T, CB), BF16),
        vm((2, NB, T, CB), BF16),
        vm((NB, T, CB), F32),
        vm((2, NT, W, 2 * FQ), BF16),
        vm((2, FF, W), BF16),
        vm((NT, 8, T), F32),
        vm((NT, 8, T), F32),
        vm((T, W), BF16),
        dma((2,)),
        dma((2,)), dma((2,)),
        dma, dma((4,)),
        dma((4, 2)), dma((4, 2)),
        dma((2, 2, 2)),
        dma((5, 2)), dma((NZ, 2)),
        dma((NZ, 2)), dma((NZ, 2)),
        dma((NZ, 2)), dma((NZ, 2)),
        dma((NZ, 2)), dma((2,)),
        dma((2, 4, 2)),
        dma((2, NB)), dma((2, NB)),
        dma,
    ]
    v = pl.BlockSpec(memory_space=pltpu.VMEM)
    a = pl.BlockSpec(memory_space=pl.ANY)
    return pl.pallas_call(
        functools.partial(layer_kernel, NP, NT),
        out_shape=jax.ShapeDtypeStruct((T, W), BF16),
        in_specs=[v, v, v, v, v, a, a, a],
        out_specs=a,
        scratch_shapes=scratch,
        compiler_params=pltpu.CompilerParams(
            collective_id=0, has_side_effects=True, vmem_limit_bytes=67043328
        ),
    )(
        tokens, routes.T, route_weights.T, norm_gain[None], final_gain[None],
        gate_weight, up_weight, down_weight,
    )


def solution(mesh):
    in_specs = (
        P("ep", "tp"),
        P("ep", None),
        P("ep", None),
        P("tp"),
        P("ep", "tp", None),
        P("ep", "tp", None),
        P("ep", None, "tp"),
        P("tp"),
    )
    out_specs = P("ep", "tp")
    return jax.shard_map(body, mesh=mesh, in_specs=in_specs, out_specs=out_specs, check_vma=False)
```

time: 195 us -> 175 us (0.90)
  Pallas kernels: 193 us -> 171 us
    pallas_call x1, Pallas kernels: 193 us -> 171 us  [body(): pl.pallas_call(functools.partial(layer_kernel, NP, NT), out_shape=jax.Sha...]
where the time goes in v3:
time: 175 us; the launch traced here: 173 us
  Pallas kernels  171 us (98%)
  local copies, waits for them, and re-layouts  2.26 us (1%)
    pallas_call x1, Pallas kernels, body(): pl.pallas_call(functools.partial(layer_kernel, NP, NT), out_shape=jax.Sha...  171 us

profile of v3, /device:TPU:36, one launch (start us, length us, event | category | flops | bytes accessed | tf_op | source)
XLA Modules:
  0.0 173.1 jit_solution(18036118697438933140)
XLA Ops:
  0.0 170.9 %shard_map.82 = bf16[512,1024]{1,0:T(8,128)(2,1)} custom-call(bf16[512,1024]{1,0:T(8,128)(2,1)} %tok.1, s32[2,512]{1,0:T(2,128)} %bitcast.4, f32[2,512]{1,0:T(2,128)} %bitcast.5, f32[1,1024]{1,0:T(1,128)} %bitcast.6, f32[1,1024]{1,0:T(1,128)} %bitcast.7, bf16[2,1024,512]{2,1,0:T(8,128)(2,1)} %gw.1, bf16[2,1024,512]{2,1,0:T(8,128)(2,1)} %uw.1, ...), custom_call_target="tpu_custom_call" | custom-call | tf_op jit(solution)/shard_map/pallas_call | solution.py:507
  170.9 2.3 %copy.10 = bf16[512,1024]{1,0:T(8,128)(2,1)} copy(bf16[512,1024]{1,0:T(8,128)(2,1)} %shard_map.82) | data formatting | bytes 2097152

commit v4 on v3

--- a/solution.py
+++ b/solution.py
@@ -15,10 +15,10 @@
 
 
 def layer_kernel(
-    NP, NT, tok, rts, rws, ngain, fgain, gw, uw, dw, out,
-    DB, MT, MR, XS, XR, PS, GS, GR, HB, OS, OR, RV, RW, CO, CM, RS, RD, ACC, WGU, WD, SQ, SQ2, OUT,
+    NP, NT, tok_hbm, rts, rws, ngain, fgain, gw, uw, dw, out,
+    DB, MT, MR, XS, XR, PS, GS, GR, HB, OS, OR, RV, RW, CO, CM, RS, RD, ACC, WGU, WD, SQ, SQ2, OUT, tok, tok_s,
     w_sem, sq_s, sq_r, mt_s, mt_r, db_s, db_r, ps_s, x_s, x_r, g_s, g_r, h_s, h_r,
-    o_s, o_r, rv_r, rd_s, rd_r, out_s,
+    o_s, o_r, rv_r, rb_r, ob_s, rd_s, rd_r, out_s,
 ):
     T, W = tok.shape
     HALF = T // 2
@@ -71,6 +71,8 @@
     for j in range(1, NT):
         pl.semaphore_signal(barrier, inc=1, device_id=tdev(j), device_id_type=MESH)
 
+    pltpu.make_async_copy(tok_hbm, tok, tok_s).start()
+    wait(tok, tok_s)
     for m in range(2):
         for q in range(NT):
             cols = pl.ds(q * FQ, FQ)
@@ -100,10 +102,10 @@
         send(part, DB.at[0, h], db_s.at[0, h], db_r.at[0, h], at_plane(1, p))
         send(part, DB.at[1, h], db_s.at[1, h], db_r.at[1, h], at_plane(-1, p))
 
+    pl.semaphore_wait(barrier, 7 * NP - 1 + NT - 1)
+    send_h(0)
     squares(lambda b: tok[b * TB:(b + 1) * TB, :].astype(F32), SQ)
-    pl.semaphore_wait(barrier, 7 * NP - 1 + NT - 1)
     share(SQ, 0)
-    send_h(0)
 
     r0 = rts[0:1, :]
     r1 = rts[1:2, :]
@@ -249,26 +251,29 @@
                 q = (p + j) % NP
                 send(OS.at[0, m, q], OR.at[m, p], o_s.at[0, m], o_r.at[m], at_plane(0, q))
             OR[m, p] = OS[0, m, p]
-        elif i < 7:
-            d = (i + 1) // 2
-            side = (i + 1) % 2
-            for j in range(1 if d == 1 else 0, NP):
-                q = (p + j) % NP
-                hop = (d - 1) * (2 * side - 1)
-                send(
-                    OS.at[i, m, q], RV.at[side, m, (d - 1) * NP + p], o_s.at[i, m],
-                    rv_r.at[side, d - 1, m], at_plane(hop, q),
-                )
-            if d == 1:
-                RV[side, m, p] = OS[i, m, p]
         else:
-            side = 1 - par
-            for j in range(NP):
-                q = (p + j) % NP
-                send(
-                    OS.at[7, m, q], RW.at[side, m, p // 2], o_s.at[7, m],
-                    rv_r.at[side, 3, m], at_plane(3 - 6 * par, q),
-                )
+            returns(i, m, 0 if i in LATE else None)
+
+    LATE = (3, 4, 7)
+
+    def returns(i, m, part):
+        cc = pl.ds(0, W) if part is None else pl.ds(part * (W // 2), W // 2)
+        d = (i + 1) // 2
+        ssem = o_s.at[i, m] if part != 1 else ob_s.at[LATE.index(i), m]
+        for j in range(1 if d == 1 else 0, NP):
+            q = (p + j) % NP
+            if i < 7:
+                side = (i + 1) % 2
+                there = at_plane((d - 1) * (2 * side - 1), q)
+                dst = RV.at[side, m, (d - 1) * NP + p, :, cc]
+            else:
+                side = 1 - par
+                there = at_plane(3 - 6 * par, q)
+                dst = RW.at[side, m, p // 2, :, cc]
+            rsem = rv_r.at[side, d - 1, m] if part != 1 else rb_r.at[side, d // 4, m]
+            send(OS.at[i, m, q, :, cc], dst, ssem, rsem, there)
+        if d == 1:
+            RV[side, m, p] = OS[i, m, p]
 
     def matrix(meta, at, b):
         bb = slice(b * TB, (b + 1) * TB)
@@ -317,12 +322,14 @@
         lax.fori_loop(0, NB, cols, 0)
 
     def relay(k):
+        cc = pl.ds(k * (W // 2), W // 2)
         for m in range(2):
             for side in range(2):
-                wait(RV.at[side, m, pl.ds(0, NP - 1)], rv_r.at[side, 0, m])
-                for d in range(1, 3):
-                    wait(RV.at[side, m, pl.ds(d * NP, NP)], rv_r.at[side, d, m])
-                wait(RW.at[side, m], rv_r.at[side, 3, m])
+                if k == 0:
+                    wait(RV.at[side, m, pl.ds(0, NP - 1)], rv_r.at[side, 0, m])
+                    wait(RV.at[side, m, pl.ds(2 * NP, NP)], rv_r.at[side, 2, m])
+                wait(RV.at[side, m, pl.ds(NP, NP), :, cc], (rb_r if k else rv_r).at[side, 1 - k, m])
+                wait(RW.at[side, m, :, :, cc], rb_r.at[side, 1, m] if k else rv_r.at[side, 3, m])
 
         def cols(n, carry):
             cc = pl.ds(pl.multiple_of(n * CB, CB), CB)
@@ -335,72 +342,79 @@
                 send(RS.at[side, n], RD.at[side, n], rd_s.at[side, n], rd_r.at[side, n], at_plane(2 * side - 1, p))
             return carry
 
-        lax.fori_loop(0, NB, cols, 0)
+        lax.fori_loop(k * NB // 2, (k + 1) * NB // 2, cols, 0)
 
     stage_a(0)
     wait(WGU, w_sem.at[0])
     stage_b(0, 0)
+    stage_c(0, 0)
+    forward(0)
     stage_b(0, 1)
-    forward(0)
-    stage_c(0, 0)
-    stage_c(0, 1)
     wait(WD, w_sem.at[1])
     stage_d(0, 0)
     stage_a(2)
+    stage_c(0, 1)
     forward(1)
+    stage_a(1)
     stage_b(2, 0)
-    stage_a(1)
     stage_b(2, 1)
     stage_d(0, 1)
+    stage_b(1, 1)
+    mats(0)
+    stage_c(2, 0)
     stage_c(2, 1)
-    stage_b(1, 1)
     stage_b(1, 0)
-    stage_c(2, 0)
     far3(0)
     far3(1)
-    stage_a(3)
+    far4(0)
+    stage_c(1, 0)
     far4(1)
     stage_c(1, 1)
-    stage_c(1, 0)
-    far4(0)
+    stage_b(5, 0)
+    stage_b(6, 0)
     stage_a(4)
-    stage_b(5, 0)
+    stage_c(5, 0)
+    stage_a(3)
+    stage_c(6, 0)
+    stage_b(5, 1)
+    stage_d(5, 0)
+    stage_b(6, 1)
+    stage_b(7, 0)
+    stage_d(6, 0)
+    stage_c(5, 1)
+    stage_c(6, 1)
+    stage_b(4, 0)
+    stage_b(7, 1)
+    stage_b(4, 1)
+    stage_d(5, 1)
+    stage_d(6, 1)
+    stage_c(7, 0)
+    stage_b(3, 1)
+    stage_d(2, 0)
     stage_d(1, 0)
-    stage_b(6, 0)
-    stage_d(1, 1)
+    stage_d(7, 0)
+    returns(7, 0, 1)
+    stage_c(4, 1)
+    stage_c(4, 0)
     stage_d(2, 1)
-    stage_c(5, 0)
-    stage_c(6, 0)
-    stage_b(6, 1)
-    stage_b(5, 1)
-    stage_d(2, 0)
-    stage_b(3, 0)
-    stage_d(5, 0)
-    stage_d(6, 0)
-    stage_c(6, 1)
-    stage_c(5, 1)
-    stage_b(7, 0)
-    stage_c(3, 0)
-    stage_b(3, 1)
-    stage_b(7, 1)
-    stage_d(6, 1)
-    stage_d(5, 1)
-    mats(0)
-    own_part(0)
-    stage_c(7, 0)
-    stage_b(4, 0)
     stage_c(3, 1)
     stage_c(7, 1)
-    stage_b(4, 1)
-    stage_d(7, 0)
+    stage_b(3, 0)
+    stage_d(4, 0)
+    own_part(0)
     stage_d(3, 1)
-    stage_c(4, 0)
     stage_d(7, 1)
-    stage_c(4, 1)
     stage_d(4, 1)
-    stage_d(4, 0)
+    returns(7, 1, 1)
+    stage_d(1, 1)
+    stage_c(3, 0)
     stage_d(3, 0)
+    returns(3, 1, 1)
+    returns(4, 0, 1)
+    returns(4, 1, 1)
+    returns(3, 0, 1)
     relay(0)
+    relay(1)
 
     def finish(n, carry):
         for side in range(2):
@@ -442,7 +456,11 @@
                 wait(XR.at[i, m, pl.ds(0, NP - 1)], x_s.at[i, m])
             wait(GR.at[i, m, pl.ds(0, NT - 1)], g_s.at[i, m])
             wait(HB.at[i, m, pl.ds(0, NT - 1)], h_s.at[i, m])
-            wait(OS.at[i, m, pl.ds(0, NP - 1)] if i <= 2 else OS.at[i, m], o_s.at[i, m])
+            if i in LATE:
+                for k, sem in enumerate((o_s.at[i, m], ob_s.at[LATE.index(i), m])):
+                    wait(OS.at[i, m, :, :, pl.ds(k * (W // 2), W // 2)], sem)
+            else:
+                wait(OS.at[i, m, pl.ds(0, NP - 1)] if i <= 2 else OS.at[i, m], o_s.at[i, m])
     wait(OUT, out_s)
 
 
@@ -489,6 +507,8 @@
         vm((NT, 8, T), F32),
         vm((NT, 8, T), F32),
         vm((T, W), BF16),
+        vm((T, W), BF16),
+        dma,
         dma((2,)),
         dma((2,)), dma((2,)),
         dma, dma((4,)),
@@ -499,6 +519,8 @@
         dma((NZ, 2)), dma((NZ, 2)),
         dma((NZ, 2)), dma((2,)),
         dma((2, 4, 2)),
+        dma((2, 2, 2)),
+        dma((3, 2)),
         dma((2, NB)), dma((2, NB)),
         dma,
     ]
@@ -507,7 +529,7 @@
     return pl.pallas_call(
         functools.partial(layer_kernel, NP, NT),
         out_shape=jax.ShapeDtypeStruct((T, W), BF16),
-        in_specs=[v, v, v, v, v, a, a, a],
+        in_specs=[a, v, v, v, v, a, a, a],
         out_specs=a,
         scratch_shapes=scratch,
         compiler_params=pltpu.CompilerParams(

time: 175 us -> 171 us (0.977)
  Pallas kernels: 171 us -> 167 us
    pallas_call x1, Pallas kernels: 171 us -> 167 us  [body(): pl.pallas_call(functools.partial(layer_kernel, NP, NT), out_shape=jax.Sha...]
where the time goes in v4:
time: 171 us; the launch traced here: 169 us
  Pallas kernels  167 us (98%)
  local copies, waits for them, and re-layouts  2.26 us (1%)
    pallas_call x1, Pallas kernels, body(): pl.pallas_call(functools.partial(layer_kernel, NP, NT), out_shape=jax.Sha...  167 us

profile of v4, /device:TPU:36, one launch (start us, length us, event | category | flops | bytes accessed | tf_op | source)
XLA Modules:
  0.0 169.1 jit_solution(4300074148846004558)
XLA Ops:
  0.0 166.8 %shard_map.82 = bf16[512,1024]{1,0:T(8,128)(2,1)} custom-call(bf16[512,1024]{1,0:T(8,128)(2,1)} %tok_hbm.1, s32[2,512]{1,0:T(2,128)} %bitcast.4, f32[2,512]{1,0:T(2,128)} %bitcast.5, f32[1,1024]{1,0:T(1,128)} %bitcast.6, f32[1,1024]{1,0:T(1,128)} %bitcast.7, bf16[2,1024,512]{2,1,0:T(8,128)(2,1)} %gw.1, bf16[2,1024,512]{2,1,0:T(8,128)(2,1)} %uw.1, ...), custom_call_target="tpu_custom_call" | custom-call | tf_op jit(solution)/shard_map/pallas_call | solution.py:529
  166.8 2.3 %copy.10 = bf16[512,1024]{1,0:T(8,128)(2,1)} copy(bf16[512,1024]{1,0:T(8,128)(2,1)} %shard_map.82) | data formatting | bytes 2097152

commit v5 on v4

--- a/solution.py
+++ b/solution.py
@@ -16,7 +16,7 @@
 
 def layer_kernel(
     NP, NT, tok_hbm, rts, rws, ngain, fgain, gw, uw, dw, out,
-    DB, MT, MR, XS, XR, PS, GS, GR, HB, OS, OR, RV, RW, CO, CM, RS, RD, ACC, WGU, WD, SQ, SQ2, OUT, tok, tok_s,
+    DB, MT, MR, XS, XR, PS, GS, GR, HB, OS, OR, RV, RW, CO, CM, RS, RD, ACC, WGU, WD, SQ, SQ2, OUT, SEL, SCA, PSQ, tok, tok_s,
     w_sem, sq_s, sq_r, mt_s, mt_r, db_s, db_r, ps_s, x_s, x_r, g_s, g_r, h_s, h_r,
     o_s, o_r, rv_r, rb_r, ob_s, rd_s, rd_r, out_s,
 ):
@@ -131,12 +131,14 @@
     near(0)
     send_h(1)
 
-    def pick(meta, at, xs, dst):
-        rows = at.shape[0]
-        s = meta[4:5, :]
+    def choose(meta, at):
         hit = (at == meta[0:1, :]) | (at == meta[1:2, :])
-        scale = jnp.sum(jnp.where(hit, s, 0.0), axis=1, keepdims=True)
-        sel = jnp.where(hit, 1.0, 0.0).astype(BF16)
+        scale = jnp.sum(jnp.where(hit, meta[4:5, :], 0.0), axis=1, keepdims=True)
+        return jnp.where(hit, 1.0, 0.0).astype(BF16), scale
+
+    def pick(meta, at, xs, dst, chosen=None):
+        sel, scale = chosen or choose(meta, at)
+        rows = sel.shape[0]
 
         def cols(n, carry):
             cc = pl.ds(pl.multiple_of(n * CB, CB), CB)
@@ -186,13 +188,19 @@
             wait_dense(k, h)
             send(DB.at[k, h], DB.at[2 + k, h], db_s.at[2 + k, h], db_r.at[2 + k, h], at_plane(1 - 2 * k, p))
 
+    chosen = {}
+
     def far3(k):
         step = 1 - 2 * k
+        if not chosen:
+            for c in range(2):
+                wait_meta(2 + c)
+                SEL[c], SCA[c] = choose(MR.at[2 + c], (row_index(RP) + zz(1 - 2 * c) * RP).astype(F32))
+                chosen[c] = True
         for h in range(2):
             wait_dense(2 + k, h)
-        wait_meta(2 + k)
         xs = (DB.at[2 + k, 0], DB.at[2 + k, 1])
-        pick(MR.at[2 + k], (row_index(RP) + zz(step) * RP).astype(F32), xs, PS.at[k, :, pl.ds(0, NP)])
+        pick(MR.at[2 + k], None, xs, PS.at[k, :, pl.ds(0, NP)], (SEL[k], SCA[k]))
         for m in range(2):
             for j in range(NP):
                 q = (p + j) % NP
@@ -419,15 +427,20 @@
     def finish(n, carry):
         for side in range(2):
             wait(RD.at[side, n], rd_r.at[side, n])
-        ACC[n] = ACC[n] + RD[0, n].astype(F32) + RD[1, n].astype(F32)
+        total = ACC[n] + RD[0, n].astype(F32) + RD[1, n].astype(F32)
+        ACC[n] = total
+        part = total * total
+        PSQ[n] = part[:, :128] + part[:, 128:] if CB == 256 else part
         return carry
 
     lax.fori_loop(0, NB, finish, 0)
 
-    def block(b):
-        return jnp.concatenate([ACC[n, b * TB:(b + 1) * TB, :] for n in range(NB)], axis=1)
-
-    squares(block, SQ2)
+    for b in range(T // TB):
+        part = PSQ[0, b * TB:(b + 1) * TB, :]
+        for n in range(1, NB):
+            part = part + PSQ[n, b * TB:(b + 1) * TB, :]
+        row = jnp.sum(part, axis=1, keepdims=True)
+        SQ2[y, :, b * TB:(b + 1) * TB] = jnp.transpose(jnp.broadcast_to(row, (TB, 128)))[0:8, :]
     share(SQ2, 1)
     wait(SQ2.at[pl.ds(0, NT - 1)], sq_r.at[1])
     final = scale_rows(SQ2)
@@ -507,6 +520,9 @@
         vm((NT, 8, T), F32),
         vm((NT, 8, T), F32),
         vm((T, W), BF16),
+        vm((2, RP, T), BF16),
+        vm((2, RP, 1), F32),
+        vm((NB, T, 128), F32),
         vm((T, W), BF16),
         dma,
         dma((2,)),

time: 171 us -> 170 us (level)
  no operation moved by 1% of the time
where the time goes in v5:
time: 170 us; the launch traced here: 168 us
  Pallas kernels  166 us (98%)
  local copies, waits for them, and re-layouts  2.26 us (1%)
    pallas_call x1, Pallas kernels, body(): pl.pallas_call(functools.partial(layer_kernel, NP, NT), out_shape=jax.Sha...  166 us

profile of v5, /device:TPU:36, one launch (start us, length us, event | category | flops | bytes accessed | tf_op | source)
XLA Modules:
  0.0 168.2 jit_solution(15326627616473649361)
XLA Ops:
  0.0 165.9 %shard_map.82 = bf16[512,1024]{1,0:T(8,128)(2,1)} custom-call(bf16[512,1024]{1,0:T(8,128)(2,1)} %tok_hbm.1, s32[2,512]{1,0:T(2,128)} %bitcast.4, f32[2,512]{1,0:T(2,128)} %bitcast.5, f32[1,1024]{1,0:T(1,128)} %bitcast.6, f32[1,1024]{1,0:T(1,128)} %bitcast.7, bf16[2,1024,512]{2,1,0:T(8,128)(2,1)} %gw.1, bf16[2,1024,512]{2,1,0:T(8,128)(2,1)} %uw.1, ...), custom_call_target="tpu_custom_call" | custom-call | tf_op jit(solution)/shard_map/pallas_call | solution.py:545
  165.9 2.3 %copy.10 = bf16[512,1024]{1,0:T(8,128)(2,1)} copy(bf16[512,1024]{1,0:T(8,128)(2,1)} %shard_map.82) | data formatting | bytes 2097152
